TPU v7x, 128 devices: a whole 4x4x4 slice. The times are simulated.
128 devices in a mesh: fs: 16 (over z, y), tp: 4 (over x), rep: 2 (over core).
Axes of the slice: x: 4, y: 4, z: 4, core: 2. Of those that a mesh axis runs over, the one named last changes fastest.
Arguments:
- gate_grads: float32 [2, 5632, 2048], P('rep', 'fs', 'tp'), may hold values from -16 to 16, as said below
- gate_velocity: float32 [5632, 2048], P(('fs', 'rep'), 'tp'), may hold values from -31 to 31, as said below
- gate_weight: float32 [5632, 2048], P(('fs', 'rep'), 'tp'), may hold values from -4 to 4
- up_grads: float32 [2, 5632, 2048], P('rep', 'fs', 'tp'), may hold values from -16 to 16, as said below
- up_velocity: float32 [5632, 2048], P(('fs', 'rep'), 'tp'), may hold values from -31 to 31, as said below
- up_weight: float32 [5632, 2048], P(('fs', 'rep'), 'tp'), may hold values from -4 to 4
- branch_grads: float32 [2, 2048, 1024], P('rep', 'fs', 'tp'), may hold values from -16 to 16, as said below
- branch_velocity: float32 [2048, 1024], P(('fs', 'rep'), 'tp'), may hold values from -31 to 31, as said below
- branch_weight: float32 [2048, 1024], P(('fs', 'rep'), 'tp'), may hold values from -4 to 4
Outputs:
- gate_momentum: float32 [5632, 2048], P(('fs', 'rep'), 'tp')
- gate_updated: float32 [5632, 2048], P(('fs', 'rep'), 'tp')
- up_momentum: float32 [5632, 2048], P(('fs', 'rep'), 'tp')
- up_updated: float32 [5632, 2048], P(('fs', 'rep'), 'tp')
- branch_momentum: float32 [2048, 1024], P(('fs', 'rep'), 'tp')
- branch_updated: float32 [2048, 1024], P(('fs', 'rep'), 'tp')
Inputs may be any that keep to these rules, and one draw needn't show every extreme that they name: `gate_grads`: entries vary in scale over rows and over columns. `up_grads`: entries vary in scale over rows and over columns. `branch_grads`: entries vary in scale over rows and over columns. `gate_velocity`: entries vary in scale over rows and over columns. `up_velocity`: entries vary in scale over rows and over columns. `branch_velocity`: entries vary in scale over rows and over columns.
All inputs are finite; a program needn't handle non-finite values.
Results may differ from a plain program's by a relative error of at most 0.039.
Values may be sent and summed in bfloat16 or wider, within the bound.
A program may use at most 64 MiB of HBM per device.

v0:
```python
import math

import jax
import jax.numpy as jnp
from jax import lax
from jax.sharding import Mesh
from jax.sharding import PartitionSpec as P

D = 2048
FF = 5632
ITERS = 3
FS_REP = ("fs_0", "fs_1", "rep")
FS_TP_REP = ("fs_0", "fs_1", "tp", "rep")
FS = ("fs_0", "fs_1")


MOMENT = 0.95
COEF_ONE = 3.4445
COEF_THREE = -4.775
COEF_FIVE = 2.0315
SAFETY = 2.0
RATE = 0.5
SHRINK = 0.95


def joined_along(tiles, dim):
    lengths = list(tiles.shape[1:])
    lengths[dim] *= tiles.shape[0]
    return jnp.moveaxis(tiles, 0, dim).reshape(lengths)


def from_everyone(value, axis):
    devices = lax.axis_size(axis)
    return lax.all_to_all(
        jnp.broadcast_to(value[None], (devices, *value.shape)), axis, 0, 0, tiled=True
    )


def gathered_copies(value, axis, dim):
    return joined_along(from_everyone(value, axis), dim)


def split_up(value, dim, devices):
    before, after = (value.shape[:dim], value.shape[dim + 1 :])
    return jnp.moveaxis(value.reshape(*before, devices, -1, *after), dim, 0)


def sum_at_owner(value, axis, dim):
    devices = lax.axis_size(axis)
    tiles = lax.all_to_all(split_up(value, dim, devices), axis, 0, 0, tiled=True)
    return jnp.sum(tiles.astype(jnp.float32), axis=0)


def by_axis(value, axes):
    for axis in axes:
        value = lax.psum(value, axis)
    return value


def side_by_side(arrays, axis, dim, along):
    ends, at = ([], 0)
    for a in arrays[:-1]:
        at += a.shape[along]
        ends.append(at)
    both = jnp.concatenate(arrays, axis=along)
    return tuple(jnp.split(sum_at_owner(both, axis, dim), ends, axis=along))


def rounded(part):
    narrow = lax.optimization_barrier(part.astype(jnp.bfloat16))
    return narrow.astype(jnp.float32)


def gram(current):
    whole = gathered_copies(current, "tp", 1)
    part = lax.dot_general(
        whole, current, (((0,), (0,)), ((), ())), preferred_element_type=jnp.float32
    )
    share = sum_at_owner(rounded(part).astype(jnp.bfloat16), FS_REP, 0)
    return (whole, share)


def spread(share):
    return lax.all_gather(share, FS_REP, axis=0, tiled=True)


def second_product(ymat, columns):
    return jnp.dot(gathered_copies(ymat, "tp", 1), columns, preferred_element_type=jnp.float32)


def combine(current, ymat, zmat, factor):
    mixed = COEF_ONE * factor * current.astype(jnp.float32) + COEF_THREE * ymat.astype(jnp.float32)
    return (mixed + COEF_FIVE * zmat.astype(jnp.float32)).astype(jnp.bfloat16)


def orthogonalize(starts):
    firsts = [gram(current) for current in starts]
    squares = tuple((jnp.sum(jnp.square(current.astype(jnp.float32))) for current in starts))
    seconds = tuple((jnp.sum(share * share) for whole, share in firsts))
    totals = jax.tree.map(lambda part: by_axis(part, FS_TP_REP), squares + seconds)
    first_sums, gram_sums = (totals[:3], totals[3:])
    finals = []
    for current, pair, first_sum, gram_sum in zip(starts, firsts, first_sums, gram_sums):
        whole, share = pair
        ratio = SAFETY * (gram_sum + 1.0) / (first_sum + 1.0)
        factor = lax.rsqrt(ratio)
        columns = spread((share / ratio).astype(jnp.bfloat16))
        ymat = (jnp.dot(whole, columns, preferred_element_type=jnp.float32) * factor).astype(
            jnp.bfloat16
        )
        zmat = second_product(ymat, columns).astype(jnp.bfloat16)
        current = combine(current, ymat, zmat, factor)
        for index in range(ITERS - 1):
            whole, share = gram(current)
            columns = spread(share.astype(jnp.bfloat16))
            ymat = jnp.dot(whole, columns, preferred_element_type=jnp.float32).astype(jnp.bfloat16)
            zmat = second_product(ymat, columns).astype(jnp.bfloat16)
            current = combine(current, ymat, zmat, 1.0)
        finals.append(current)
    return tuple(finals)


def local(
    gate_grads,
    gate_velocity,
    gate_weight,
    up_grads,
    up_velocity,
    up_weight,
    branch_grads,
    branch_velocity,
    branch_weight,
):
    totals = (
        *side_by_side(
            (gate_grads.astype(jnp.bfloat16), up_grads.astype(jnp.bfloat16)), "rep", 1, 0
        ),
        sum_at_owner(branch_grads.astype(jnp.bfloat16), "rep", 1),
    )
    velocities = (gate_velocity, up_velocity, branch_velocity)
    moments = [MOMENT * velocity + total[0] for velocity, total in zip(velocities, totals)]
    starts = tuple((moment.astype(jnp.bfloat16) for moment in moments))
    finals = orthogonalize(starts)
    weights = (gate_weight, up_weight, branch_weight)
    heights = (FF, FF, D)
    results = []
    for moment, weight, final, height in zip(moments, weights, finals, heights):
        results.append(moment)
        results.append(SHRINK * weight - RATE * math.sqrt(height) * final.astype(jnp.float32))
    return tuple(results)


def solution(mesh):
    torus = Mesh(
        mesh.devices.reshape(4, 4, mesh.shape["tp"], mesh.shape["rep"]),
        ("fs_0", "fs_1", "tp", "rep"),
    )
    return jax.shard_map(
        local,
        mesh=torus,
        in_specs=(
            P("rep", FS, "tp"),
            P(FS_REP, "tp"),
            P(FS_REP, "tp"),
            P("rep", FS, "tp"),
            P(FS_REP, "tp"),
            P(FS_REP, "tp"),
            P("rep", FS, "tp"),
            P(FS_REP, "tp"),
            P(FS_REP, "tp"),
        ),
        out_specs=(
            P(FS_REP, "tp"),
            P(FS_REP, "tp"),
            P(FS_REP, "tp"),
            P(FS_REP, "tp"),
            P(FS_REP, "tp"),
            P(FS_REP, "tp"),
        ),
        check_vma=False,
    )
```

profile of v0, /device:TPU:1, one launch (start us, length us, event | category | flops | bytes accessed | tf_op | source)
XLA Modules:
  0.0 690.4 jit_solution(9970207772940206711)
XLA Ops:
  31.5 12.0 %all_to_all.145 = bf16[4,176,512]{2,1,0:T(8,128)(2,1)S(1)} all-to-all(bf16[4,176,512]{2,1,0:T(8,128)(2,1)S(1)} %broadcast_in_dim.42), channel_id=1, replica_groups=mesh['fs_0'=4,'fs_1'=4,'tp'=4,'rep'=2] {'tp'}, dimensions={0} | all-to-all | bytes 1441792 | tf_op jit(solution)/shard_map/all_to_all | solution.py:34
  49.1 7.2 %all-to-all-done.1 = bf16[4,176,512]{2,1,0:T(8,128)(2,1)S(1)} async-done(((bf16[4,176,512]{2,1,0:T(8,128)(2,1)}), bf16[4,176,512]{2,1,0:T(8,128)(2,1)S(1)}, u32[]{:S(2)}, u32[]{:S(2)}) %all-to-all-start.1) | async-done | bytes 720928 | tf_op jit(solution)/shard_map/all_to_all | solution.py:34
  56.3 12.2 %all-to-all-start.21 = ((bf16[32,32,256]{2,1,0:T(8,128)(2,1)}), bf16[32,32,256]{2,1,0:T(8,128)(2,1)S(1)}, u32[]{:S(2)}, u32[]{:S(2)}) async-start(bf16[32,32,256]{2,1,0:T(8,128)(2,1)} %bitcast.24), calls=%async_computation.21 | async-start | bytes 1048576 | tf_op jit(solution)/shard_map/all_to_all | solution.py:50
  70.7 9.3 %all-to-all-done.21 = bf16[32,32,256]{2,1,0:T(8,128)(2,1)S(1)} async-done(((bf16[32,32,256]{2,1,0:T(8,128)(2,1)}), bf16[32,32,256]{2,1,0:T(8,128)(2,1)S(1)}, u32[]{:S(2)}, u32[]{:S(2)}) %all-to-all-start.21) | async-done | bytes 524320 | tf_op jit(solution)/shard_map/all_to_all | solution.py:50
  89.1 24.1 %all-to-all-done.11 = bf16[32,64,512]{2,1,0:T(8,128)(2,1)S(1)} async-done(((bf16[32,64,512]{2,1,0:T(8,128)(2,1)}), bf16[32,64,512]{2,1,0:T(8,128)(2,1)S(1)}, u32[]{:S(2)}, u32[]{:S(2)}) %all-to-all-start.11) | async-done | bytes 2097184 | tf_op jit(solution)/shard_map/all_to_all | solution.py:50
  123.7 24.3 %all-to-all-done.2 = bf16[32,64,512]{2,1,0:T(8,128)(2,1)} async-done(((bf16[32,64,512]{2,1,0:T(8,128)(2,1)}), bf16[32,64,512]{2,1,0:T(8,128)(2,1)}, u32[]{:S(2)}, u32[]{:S(2)}) %all-to-all-start.2) | async-done | bytes 2097184 | tf_op jit(solution)/shard_map/all_to_all | solution.py:50
  157.7 9.9 %all-reduce.1 = (f32[]{:T(128)}, f32[]{:T(128)}, f32[]{:T(128)}, f32[]{:T(128)}, f32[]{:T(128)}, /*index=5*/f32[]{:T(128)}) all-reduce(f32[]{:T(128)} %get-tuple-element.18, f32[]{:T(128)} %get-tuple-element.19, f32[]{:T(128)} %get-tuple-element.20, f32[]{:T(128)} %get-tuple-element.21, ...), channel_id=1, replica_groups=mesh['fs_0'=4,'fs_1'=4,'tp'=4,'rep'=2] {'fs_1'}, use_global_device_ids=true, to_apply=%region_4.0 | all-reduce | flops 6 | bytes 48 | tf_op jit(solution)/shard_map/psum | solution.py:56
  167.6 7.6 %all-reduce = (f32[]{:T(128)}, f32[]{:T(128)}, f32[]{:T(128)}, f32[]{:T(128)}, f32[]{:T(128)}, /*index=5*/f32[]{:T(128)}) all-reduce(f32[]{:T(128)} %get-tuple-element.12, f32[]{:T(128)} %get-tuple-element.13, f32[]{:T(128)} %get-tuple-element.14, f32[]{:T(128)} %get-tuple-element.15, ...), channel_id=1, replica_groups=mesh['fs_0'=4,'fs_1'=4,'tp'=4,'rep'=2] {'tp'}, use_global_device_ids=true, to_apply=%region_5.0 | all-reduce | flops 6 | bytes 48 | tf_op jit(solution)/shard_map/psum | solution.py:56
  175.2 8.0 %all-reduce.3 = (f32[]{:T(128)}, f32[]{:T(128)}, f32[]{:T(128)}, f32[]{:T(128)}, f32[]{:T(128)}, /*index=5*/f32[]{:T(128)}) all-reduce(f32[]{:T(128)} %get-tuple-element.6, f32[]{:T(128)} %get-tuple-element.7, f32[]{:T(128)} %get-tuple-element.8, f32[]{:T(128)} %get-tuple-element.9, ...), channel_id=1, replica_groups=mesh['fs_0'=4,'fs_1'=4,'tp'=4,'rep'=2] {'rep'}, use_global_device_ids=true, to_apply=%region_6.0 | all-reduce | flops 6 | bytes 48 | tf_op jit(solution)/shard_map/psum | solution.py:56
  187.1 37.8 %all-gather.13.cloned.1.call-done = bf16[2048,512]{1,0:T(8,128)(2,1)} async-done(((bf16[64,512]{1,0:T(8,128)(2,1)}), bf16[2048,512]{1,0:T(8,128)(2,1)}) %all-gather.13.cloned.1.call-update) | async-done | bytes 2097168 | tf_op jit(solution)/shard_map/all_gather | solution.py:84
  232.0 11.1 %all-to-all-done.12 = bf16[4,176,512]{2,1,0:T(8,128)(2,1)S(1)} async-done(((bf16[4,176,512]{2,1,0:T(8,128)(2,1)}), bf16[4,176,512]{2,1,0:T(8,128)(2,1)S(1)}, u32[]{:S(2)}, u32[]{:S(2)}) %all-to-all-start.12) | async-done | bytes 720928 | tf_op jit(solution)/shard_map/all_to_all | solution.py:34
  245.4 12.6 %all_to_all.146 = bf16[4,176,512]{2,1,0:T(8,128)(2,1)S(1)} all-to-all(bf16[4,176,512]{2,1,0:T(8,128)(2,1)S(1)} %broadcast_in_dim.44), channel_id=1, replica_groups=mesh['fs_0'=4,'fs_1'=4,'tp'=4,'rep'=2] {'tp'}, dimensions={0} | all-to-all | bytes 1441792 | tf_op jit(solution)/shard_map/all_to_all | solution.py:34
  258.9 35.4 %all_to_all.147 = bf16[32,64,512]{2,1,0:T(8,128)(2,1)S(1)} all-to-all(bf16[32,64,512]{2,1,0:T(8,128)(2,1)S(1)} %bitcast.134), channel_id=1, replica_groups=mesh['fs_0'=4,'fs_1'=4,'tp'=4,'rep'=2] {'fs_0','fs_1','rep'}, dimensions={0} | all-to-all | bytes 4194304 | tf_op jit(solution)/shard_map/all_to_all | solution.py:50
  302.6 11.2 %all-to-all-done.3 = bf16[4,176,512]{2,1,0:T(8,128)(2,1)S(1)} async-done(((bf16[4,176,512]{2,1,0:T(8,128)(2,1)}), bf16[4,176,512]{2,1,0:T(8,128)(2,1)S(1)}, u32[]{:S(2)}, u32[]{:S(2)}) %all-to-all-start.3) | async-done | bytes 720928 | tf_op jit(solution)/shard_map/all_to_all | solution.py:34
  315.5 12.7 %all_to_all.148 = bf16[4,176,512]{2,1,0:T(8,128)(2,1)S(1)} all-to-all(bf16[4,176,512]{2,1,0:T(8,128)(2,1)S(1)} %broadcast_in_dim.38), channel_id=1, replica_groups=mesh['fs_0'=4,'fs_1'=4,'tp'=4,'rep'=2] {'tp'}, dimensions={0} | all-to-all | bytes 1441792 | tf_op jit(solution)/shard_map/all_to_all | solution.py:34
  329.2 34.6 %all_to_all.149 = bf16[32,64,512]{2,1,0:T(8,128)(2,1)S(1)} all-to-all(bf16[32,64,512]{2,1,0:T(8,128)(2,1)S(1)} %bitcast.135), channel_id=1, replica_groups=mesh['fs_0'=4,'fs_1'=4,'tp'=4,'rep'=2] {'fs_0','fs_1','rep'}, dimensions={0} | all-to-all | bytes 4194304 | tf_op jit(solution)/shard_map/all_to_all | solution.py:50
  367.2 13.5 %all_to_all.150 = bf16[4,176,512]{2,1,0:T(8,128)(2,1)S(1)} all-to-all(bf16[4,176,512]{2,1,0:T(8,128)(2,1)S(1)} %broadcast_in_dim.45), channel_id=1, replica_groups=mesh['fs_0'=4,'fs_1'=4,'tp'=4,'rep'=2] {'tp'}, dimensions={0} | all-to-all | bytes 1441792 | tf_op jit(solution)/shard_map/all_to_all | solution.py:34
  381.5 12.5 %all_to_all.151 = bf16[4,176,512]{2,1,0:T(8,128)(2,1)S(1)} all-to-all(bf16[4,176,512]{2,1,0:T(8,128)(2,1)S(1)} %broadcast_in_dim.46), channel_id=1, replica_groups=mesh['fs_0'=4,'fs_1'=4,'tp'=4,'rep'=2] {'tp'}, dimensions={0} | all-to-all | bytes 1441792 | tf_op jit(solution)/shard_map/all_to_all | solution.py:34
  394.9 35.2 %all_to_all.152 = bf16[32,64,512]{2,1,0:T(8,128)(2,1)S(1)} all-to-all(bf16[32,64,512]{2,1,0:T(8,128)(2,1)S(1)} %bitcast.136), channel_id=1, replica_groups=mesh['fs_0'=4,'fs_1'=4,'tp'=4,'rep'=2] {'fs_0','fs_1','rep'}, dimensions={0} | all-to-all | bytes 4194304 | tf_op jit(solution)/shard_map/all_to_all | solution.py:50
  433.4 13.5 %all_to_all.153 = bf16[4,176,512]{2,1,0:T(8,128)(2,1)S(1)} all-to-all(bf16[4,176,512]{2,1,0:T(8,128)(2,1)S(1)} %broadcast_in_dim.39), channel_id=1, replica_groups=mesh['fs_0'=4,'fs_1'=4,'tp'=4,'rep'=2] {'tp'}, dimensions={0} | all-to-all | bytes 1441792 | tf_op jit(solution)/shard_map/all_to_all | solution.py:34
  447.7 12.5 %all_to_all.154 = bf16[4,176,512]{2,1,0:T(8,128)(2,1)S(1)} all-to-all(bf16[4,176,512]{2,1,0:T(8,128)(2,1)S(1)} %broadcast_in_dim.40), channel_id=1, replica_groups=mesh['fs_0'=4,'fs_1'=4,'tp'=4,'rep'=2] {'tp'}, dimensions={0} | all-to-all | bytes 1441792 | tf_op jit(solution)/shard_map/all_to_all | solution.py:34
  462.3 7.2 %all-to-all-start.8 = ((bf16[32,64,512]{2,1,0:T(8,128)(2,1)}), bf16[32,64,512]{2,1,0:T(8,128)(2,1)S(1)}, u32[]{:S(2)}, u32[]{:S(2)}) async-start(bf16[32,64,512]{2,1,0:T(8,128)(2,1)} %bitcast.131), calls=%async_computation.8 | async-start | bytes 4194304 | tf_op jit(solution)/shard_map/all_to_all | solution.py:50
  470.9 27.2 %all-to-all-done.8 = bf16[32,64,512]{2,1,0:T(8,128)(2,1)S(1)} async-done(((bf16[32,64,512]{2,1,0:T(8,128)(2,1)}), bf16[32,64,512]{2,1,0:T(8,128)(2,1)S(1)}, u32[]{:S(2)}, u32[]{:S(2)}) %all-to-all-start.8) | async-done | bytes 2097184 | tf_op jit(solution)/shard_map/all_to_all | solution.py:50
  499.9 23.3 %all_gather.33 = bf16[1024,256]{1,0:T(8,128)(2,1)S(1)} all-gather(bf16[32,256]{1,0:T(8,128)(2,1)S(1)} %divide_convert_fusion.2), channel_id=1, replica_groups=mesh['fs_0'=4,'fs_1'=4,'tp'=4,'rep'=2] {'fs_0','fs_1','rep'}, dimensions={0}, use_global_device_ids=true | all-gather | bytes 540672 | tf_op jit(solution)/shard_map/all_gather | solution.py:84
  534.2 7.2 %all_to_all.155 = bf16[4,64,256]{2,1,0:T(8,128)(2,1)S(1)} all-to-all(bf16[4,64,256]{2,1,0:T(8,128)(2,1)S(1)} %broadcast_in_dim.50), channel_id=1, replica_groups=mesh['fs_0'=4,'fs_1'=4,'tp'=4,'rep'=2] {'tp'}, dimensions={0} | all-to-all | bytes 262144 | tf_op jit(solution)/shard_map/all_to_all | solution.py:34
  541.8 19.2 %all_to_all.156 = bf16[32,32,256]{2,1,0:T(8,128)(2,1)S(1)} all-to-all(bf16[32,32,256]{2,1,0:T(8,128)(2,1)S(1)} %bitcast.164), channel_id=1, replica_groups=mesh['fs_0'=4,'fs_1'=4,'tp'=4,'rep'=2] {'fs_0','fs_1','rep'}, dimensions={0} | all-to-all | bytes 1048576 | tf_op jit(solution)/shard_map/all_to_all | solution.py:50
  561.1 22.8 %all_gather.34 = bf16[1024,256]{1,0:T(8,128)(2,1)S(1)} all-gather(bf16[32,256]{1,0:T(8,128)(2,1)S(1)} %reduce_sum.186), channel_id=1, replica_groups=mesh['fs_0'=4,'fs_1'=4,'tp'=4,'rep'=2] {'fs_0','fs_1','rep'}, dimensions={0}, use_global_device_ids=true | all-gather | bytes 540672 | tf_op jit(solution)/shard_map/all_gather | solution.py:84
  584.1 7.3 %all_to_all.157 = bf16[4,64,256]{2,1,0:T(8,128)(2,1)S(1)} all-to-all(bf16[4,64,256]{2,1,0:T(8,128)(2,1)S(1)} %broadcast_in_dim.51), channel_id=1, replica_groups=mesh['fs_0'=4,'fs_1'=4,'tp'=4,'rep'=2] {'tp'}, dimensions={0} | all-to-all | bytes 262144 | tf_op jit(solution)/shard_map/all_to_all | solution.py:34
  591.7 7.2 %all_to_all.158 = bf16[4,64,256]{2,1,0:T(8,128)(2,1)S(1)} all-to-all(bf16[4,64,256]{2,1,0:T(8,128)(2,1)S(1)} %broadcast_in_dim.52), channel_id=1, replica_groups=mesh['fs_0'=4,'fs_1'=4,'tp'=4,'rep'=2] {'tp'}, dimensions={0} | all-to-all | bytes 262144 | tf_op jit(solution)/shard_map/all_to_all | solution.py:34
  599.3 18.4 %all_to_all.159 = bf16[32,32,256]{2,1,0:T(8,128)(2,1)S(1)} all-to-all(bf16[32,32,256]{2,1,0:T(8,128)(2,1)S(1)} %bitcast.165), channel_id=1, replica_groups=mesh['fs_0'=4,'fs_1'=4,'tp'=4,'rep'=2] {'fs_0','fs_1','rep'}, dimensions={0} | all-to-all | bytes 1048576 | tf_op jit(solution)/shard_map/all_to_all | solution.py:50
  617.8 23.0 %all_gather.35 = bf16[1024,256]{1,0:T(8,128)(2,1)S(1)} all-gather(bf16[32,256]{1,0:T(8,128)(2,1)S(1)} %reduce_sum.187), channel_id=1, replica_groups=mesh['fs_0'=4,'fs_1'=4,'tp'=4,'rep'=2] {'fs_0','fs_1','rep'}, dimensions={0}, use_global_device_ids=true | all-gather | bytes 540672 | tf_op jit(solution)/shard_map/all_gather | solution.py:84
  657.4 8.1 %all-to-all-done.18 = bf16[4,176,512]{2,1,0:T(8,128)(2,1)S(1)} async-done(((bf16[4,176,512]{2,1,0:T(8,128)(2,1)}), bf16[4,176,512]{2,1,0:T(8,128)(2,1)S(1)}, u32[]{:S(2)}, u32[]{:S(2)}) %all-to-all-start.18) | async-done | bytes 720928 | tf_op jit(solution)/shard_map/all_to_all | solution.py:34
  (203 shorter events, 143.0 us)
Async XLA Ops:
  8.7 8.0 %all-to-all-start.19 = ((bf16[2,1,64,256]{3,2,1,0:T(8,128)(2,1)}), bf16[2,1,64,256]{3,2,1,0:T(8,128)(2,1)S(1)}, u32[]{:S(2)}, u32[]{:S(2)}) async-start(bf16[2,1,64,256]{3,2,1,0:T(8,128)(2,1)} %bitcast.22), calls=%async_computation.19 | async-start | bytes 131072 | tf_op jit(solution)/shard_map/all_to_all | solution.py:50
  16.7 5.2 all-to-all-start
  21.6 26.3 %copy-start.31 = (bf16[64,256]{1,0:T(8,128)(2,1)}, bf16[64,256]{1,0:T(8,128)(2,1)S(1)}, u32[]{:S(2)}) copy-start(bf16[64,256]{1,0:T(8,128)(2,1)S(1)} %get-tuple-element.31) | copy-start | bytes 98308
  22.5 9.0 %all-to-all-start.20 = ((bf16[4,64,256]{2,1,0:T(8,128)(2,1)}), bf16[4,64,256]{2,1,0:T(8,128)(2,1)S(1)}, u32[]{:S(2)}, u32[]{:S(2)}) async-start(bf16[4,64,256]{2,1,0:T(8,128)(2,1)} %broadcast_in_dim.48), calls=%async_computation.20 | async-start | bytes 262144 | tf_op jit(solution)/shard_map/all_to_all | solution.py:34
  28.5 16.0 %copy-start.12 = (bf16[176,512]{1,0:T(8,128)(2,1)}, bf16[176,512]{1,0:T(8,128)(2,1)S(1)}, u32[]{:S(2)}) copy-start(bf16[176,512]{1,0:T(8,128)(2,1)S(1)} %get-tuple-element.40) | copy-start | bytes 540676
  28.5 40.2 %copy-start.13 = (bf16[176,512]{1,0:T(8,128)(2,1)}, bf16[176,512]{1,0:T(8,128)(2,1)S(1)}, u32[]{:S(2)}) copy-start(bf16[176,512]{1,0:T(8,128)(2,1)S(1)} %get-tuple-element.34) | copy-start | bytes 540676
  44.4 11.9 %all-to-all-start.1 = ((bf16[4,176,512]{2,1,0:T(8,128)(2,1)}), bf16[4,176,512]{2,1,0:T(8,128)(2,1)S(1)}, u32[]{:S(2)}, u32[]{:S(2)}) async-start(bf16[4,176,512]{2,1,0:T(8,128)(2,1)} %broadcast_in_dim.36), calls=%async_computation.1 | async-start | bytes 1441792 | tf_op jit(solution)/shard_map/all_to_all | solution.py:34
  56.3 14.4 %copy-start.6 = (bf16[4,176,512]{2,1,0:T(8,128)(2,1)}, bf16[4,176,512]{2,1,0:T(8,128)(2,1)S(1)}, u32[]{:S(2)}) copy-start(bf16[4,176,512]{2,1,0:T(8,128)(2,1)S(1)} %all-to-all-done.1) | copy-start | bytes 2162692
  56.3 23.6 %all-to-all-start.21 = ((bf16[32,32,256]{2,1,0:T(8,128)(2,1)}), bf16[32,32,256]{2,1,0:T(8,128)(2,1)S(1)}, u32[]{:S(2)}, u32[]{:S(2)}) async-start(bf16[32,32,256]{2,1,0:T(8,128)(2,1)} %bitcast.24), calls=%async_computation.21 | async-start | bytes 1048576 | tf_op jit(solution)/shard_map/all_to_all | solution.py:50
  80.8 32.4 %all-to-all-start.11 = ((bf16[32,64,512]{2,1,0:T(8,128)(2,1)}), bf16[32,64,512]{2,1,0:T(8,128)(2,1)S(1)}, u32[]{:S(2)}, u32[]{:S(2)}) async-start(bf16[32,64,512]{2,1,0:T(8,128)(2,1)} %bitcast.133), calls=%async_computation.11 | async-start | bytes 4194304 | tf_op jit(solution)/shard_map/all_to_all | solution.py:50
  113.2 34.9 %all-to-all-start.2 = ((bf16[32,64,512]{2,1,0:T(8,128)(2,1)}), bf16[32,64,512]{2,1,0:T(8,128)(2,1)}, u32[]{:S(2)}, u32[]{:S(2)}) async-start(bf16[32,64,512]{2,1,0:T(8,128)(2,1)} %bitcast.132), calls=%async_computation.2 | async-start | bytes 4194304 | tf_op jit(solution)/shard_map/all_to_all | solution.py:50
  119.7 105.3 %all-gather.13.cloned.1.call-start = ((), (), s32[]{:S(2)}) async-start(), calls=%async_computation.32 | async-start | bytes 2162688 | tf_op jit(solution)/shard_map/all_gather | solution.py:84
  123.7 60.8 %copy-start.23 = (f32[64,512]{1,0:T(8,128)S(1)}, f32[64,512]{1,0:T(8,128)}, u32[]{:S(2)}) copy-start(f32[64,512]{1,0:T(8,128)} %copy-done.22) | copy-start | bytes 393220
  185.1 110.2 %all-gather.7.cloned.1.call-start = ((), (), s32[]{:S(2)}) async-start(), calls=%async_computation.29 | async-start | bytes 2162688 | tf_op jit(solution)/shard_map/all_gather | solution.py:84
  227.1 16.1 %copy-start.14 = (bf16[176,512]{1,0:T(8,128)(2,1)S(1)}, bf16[176,512]{1,0:T(8,128)(2,1)}, u32[]{:S(2)}) copy-start(bf16[176,512]{1,0:T(8,128)(2,1)} %copy-done.13) | copy-start | bytes 540676
  228.0 15.1 %all-to-all-start.12 = ((bf16[4,176,512]{2,1,0:T(8,128)(2,1)}), bf16[4,176,512]{2,1,0:T(8,128)(2,1)S(1)}, u32[]{:S(2)}, u32[]{:S(2)}) async-start(bf16[4,176,512]{2,1,0:T(8,128)(2,1)} %broadcast_in_dim.43), calls=%async_computation.12 | async-start | bytes 1441792 | tf_op jit(solution)/shard_map/all_to_all | solution.py:34
  232.0 133.0 %all-gather.15.cloned.1.call-start = ((), (), s32[]{:S(2)}) async-start(), calls=%async_computation.33 | async-start | bytes 2162688 | tf_op jit(solution)/shard_map/all_gather | solution.py:84
  298.2 15.7 %copy-start.8 = (bf16[2048,512]{1,0:T(8,128)(2,1)S(1)}, bf16[2048,512]{1,0:T(8,128)(2,1)}, u32[]{:S(2)}) copy-start(bf16[2048,512]{1,0:T(8,128)(2,1)} %all-gather.7.cloned.1.call-done) | copy-start | bytes 6291460
  299.1 14.7 %all-to-all-start.3 = ((bf16[4,176,512]{2,1,0:T(8,128)(2,1)}), bf16[4,176,512]{2,1,0:T(8,128)(2,1)S(1)}, u32[]{:S(2)}, u32[]{:S(2)}) async-start(bf16[4,176,512]{2,1,0:T(8,128)(2,1)} %broadcast_in_dim.37), calls=%async_computation.3 | async-start | bytes 1441792 | tf_op jit(solution)/shard_map/all_to_all | solution.py:34
  302.6 128.5 %all-gather.9.cloned.1.call-start = ((), (), s32[]{:S(2)}) async-start(), calls=%async_computation.30 | async-start | bytes 2162688 | tf_op jit(solution)/shard_map/all_gather | solution.py:84
  364.8 281.1 %all-gather.17.cloned.1.call-start = ((), (), s32[]{:S(2)}) async-start(), calls=%async_computation.34 | async-start | bytes 2162688 | tf_op jit(solution)/shard_map/all_gather | solution.py:84
  433.4 13.7 %copy-start.10 = (bf16[2048,512]{1,0:T(8,128)(2,1)S(1)}, bf16[2048,512]{1,0:T(8,128)(2,1)}, u32[]{:S(2)}) copy-start(bf16[2048,512]{1,0:T(8,128)(2,1)} %all-gather.9.cloned.1.call-done) | copy-start | bytes 6291460
  447.6 14.7 %copy-start.17 = (bf16[176,512]{1,0:T(8,128)(2,1)}, bf16[176,512]{1,0:T(8,128)(2,1)S(1)}, u32[]{:S(2)}) copy-start(bf16[176,512]{1,0:T(8,128)(2,1)S(1)} %fusion.21) | copy-start | bytes 540676
  462.3 35.8 %all-to-all-start.8 = ((bf16[32,64,512]{2,1,0:T(8,128)(2,1)}), bf16[32,64,512]{2,1,0:T(8,128)(2,1)S(1)}, u32[]{:S(2)}, u32[]{:S(2)}) async-start(bf16[32,64,512]{2,1,0:T(8,128)(2,1)} %bitcast.131), calls=%async_computation.8 | async-start | bytes 4194304 | tf_op jit(solution)/shard_map/all_to_all | solution.py:50
  469.5 185.7 %all-gather.11.cloned.1.call-start = ((), (), s32[]{:S(2)}) async-start(), calls=%async_computation.31 | async-start | bytes 2162688 | tf_op jit(solution)/shard_map/all_gather | solution.py:84
  525.0 8.2 %all-to-all-start.22 = ((bf16[4,64,256]{2,1,0:T(8,128)(2,1)}), bf16[4,64,256]{2,1,0:T(8,128)(2,1)S(1)}, u32[]{:S(2)}, u32[]{:S(2)}) async-start(bf16[4,64,256]{2,1,0:T(8,128)(2,1)} %broadcast_in_dim.49), calls=%async_computation.22 | async-start | bytes 262144 | tf_op jit(solution)/shard_map/all_to_all | solution.py:34
  591.7 50.1 %copy-start.32 = (bf16[64,256]{1,0:T(8,128)(2,1)}, bf16[64,256]{1,0:T(8,128)(2,1)S(1)}, u32[]{:S(2)}) copy-start(bf16[64,256]{1,0:T(8,128)(2,1)S(1)} %fusion.43) | copy-start | bytes 98308
  642.5 8.2 %all-to-all-start.28 = ((bf16[4,64,256]{2,1,0:T(8,128)(2,1)}), bf16[4,64,256]{2,1,0:T(8,128)(2,1)S(1)}, u32[]{:S(2)}, u32[]{:S(2)}) async-start(bf16[4,64,256]{2,1,0:T(8,128)(2,1)} %broadcast_in_dim.53), calls=%async_computation.28 | async-start | bytes 262144 | tf_op jit(solution)/shard_map/all_to_all | solution.py:34
  651.7 13.9 %all-to-all-start.18 = ((bf16[4,176,512]{2,1,0:T(8,128)(2,1)}), bf16[4,176,512]{2,1,0:T(8,128)(2,1)S(1)}, u32[]{:S(2)}, u32[]{:S(2)}) async-start(bf16[4,176,512]{2,1,0:T(8,128)(2,1)} %broadcast_in_dim.47), calls=%async_computation.18 | async-start | bytes 1441792 | tf_op jit(solution)/shard_map/all_to_all | solution.py:34
  655.2 16.1 %copy-start.5 = (bf16[1024,256]{1,0:T(8,128)(2,1)S(1)}, bf16[1024,256]{1,0:T(8,128)(2,1)}, u32[]{:S(2)}) copy-start(bf16[1024,256]{1,0:T(8,128)(2,1)} %copy-done.4) | copy-start | bytes 1572868
  657.4 13.8 %copy-start.38 = (bf16[64,256]{1,0:T(8,128)(2,1)S(1)}, bf16[64,256]{1,0:T(8,128)(2,1)}, u32[]{:S(2)}) copy-start(bf16[64,256]{1,0:T(8,128)(2,1)} %copy-done.37) | copy-start | bytes 98308
  666.7 12.7 %all-to-all-start.9 = ((bf16[4,176,512]{2,1,0:T(8,128)(2,1)}), bf16[4,176,512]{2,1,0:T(8,128)(2,1)S(1)}, u32[]{:S(2)}, u32[]{:S(2)}) async-start(bf16[4,176,512]{2,1,0:T(8,128)(2,1)} %broadcast_in_dim.41), calls=%async_computation.9 | async-start | bytes 1441792 | tf_op jit(solution)/shard_map/all_to_all | solution.py:34
  (28 other events, 175.1 us)
Sparse Core Ops, SparseCore 0:
  185.3 39.6 all-gather.12
  227.8 42.9 all-gather.6
  295.4 40.0 all-gather.14
  364.9 39.7 all-gather.8
  431.2 39.7 all-gather.16
  499.2 40.6 all-gather.10
where the time goes:
time: 695 us; the launch traced here: 690 us
  blocking collectives  356 us (51%)
  waiting for transfers between devices  176 us (25%)
  starting transfers between devices  67.3 us (10%)
  matrix products  37.3 us (5%)
  between operations  19 us (3%)
  other arithmetic  18.2 us (3%)
  local copies, waits for them, and re-layouts  17.1 us (2%)
    all_to_all x5, blocking collectives, sum_at_owner(): lax.all_to_all(split_up(value, dim, devices), axis, 0, 0, tiled=True)  143 us
    all_to_all x10, blocking collectives, from_everyone(): lax.all_to_all(jnp.broadcast_to(value[None], (devices, *value.shape)), ax...  111 us
    all_to_all x6, waiting for transfers between devices, sum_at_owner(): lax.all_to_all(split_up(value, dim, devices), axis, 0, 0, tiled=True)  85.1 us
    all_gather x3, blocking collectives, spread(): return lax.all_gather(share, FS_REP, axis=0, tiled=True)  69.1 us
    all_to_all x8, waiting for transfers between devices, from_everyone(): lax.all_to_all(jnp.broadcast_to(value[None], (devices, *value.shape)), ax...  52.6 us
    all_to_all x6, starting transfers between devices, sum_at_owner(): lax.all_to_all(split_up(value, dim, devices), axis, 0, 0, tiled=True)  38.2 us
    all_gather x6, waiting for transfers between devices, spread(): return lax.all_gather(share, FS_REP, axis=0, tiled=True)  37.9 us
    psum x4, blocking collectives, by_axis(): value = lax.psum(value, axis)  32.6 us
  transfers between devices with their start and end apart: 20, of which 14 were waited for; matrix products, arithmetic and copies ran while one was open for 8% of the time, Pallas kernels for 0%

commit v1 on v0

v1 whole, which is shorter than its diff:
```python
import math

import jax
import jax.numpy as jnp
from jax import lax
from jax.sharding import Mesh
from jax.sharding import PartitionSpec as P

D = 2048
FF = 5632
FS_REP = ("fs_0", "fs_1", "rep")
FS = ("fs_0", "fs_1")

MOMENT = 0.95
COEF_ONE = 3.4445
COEF_THREE = -4.775
COEF_FIVE = 2.0315
SAFETY = 2.0
RATE = 0.5
SHRINK = 0.95
BF = jnp.bfloat16


def dot(a, b):
    return jnp.dot(a, b, preferred_element_type=jnp.float32)


def sum_at_owner(value, axis, dim):
    devices = lax.axis_size(axis)
    before, after = (value.shape[:dim], value.shape[dim + 1 :])
    tiles = jnp.moveaxis(value.reshape(*before, devices, -1, *after), dim, 0)
    tiles = lax.all_to_all(tiles, axis, 0, 0, tiled=True)
    return jnp.sum(tiles.astype(jnp.float32), axis=0)


def chain(raw, start):
    raw = raw.astype(jnp.float32)
    ratio = SAFETY * (jnp.sum(raw * raw) + 1.0) / (jnp.trace(raw) + 1.0)
    scale = lax.rsqrt(ratio)
    g = (raw / ratio).astype(BF)
    x, factor = start, scale
    for index in range(3):
        s = dot(g, g)
        m = (COEF_THREE * g.astype(jnp.float32) + COEF_FIVE * s).astype(BF)
        if index == 2:
            return x, m
        t = (COEF_ONE * g.astype(jnp.float32) + dot(g, m)).astype(BF)
        x = (factor * (COEF_ONE * x.astype(jnp.float32) + dot(x, m))).astype(BF)
        g = (COEF_ONE * t.astype(jnp.float32) + dot(t, m)).astype(BF)
        factor = 1.0


def last(x, m, column, width):
    own = lax.dynamic_slice_in_dim(x, column * width, width, 1)
    cols = lax.dynamic_slice_in_dim(m, column * width, width, 1)
    return (COEF_ONE * own.astype(jnp.float32) + dot(x, cols)).astype(BF)


def local(
    gate_grads,
    gate_velocity,
    gate_weight,
    up_grads,
    up_velocity,
    up_weight,
    branch_grads,
    branch_velocity,
    branch_weight,
):
    both = jnp.concatenate((gate_grads.astype(BF), up_grads.astype(BF)), axis=0)
    total = sum_at_owner(both, "rep", 1)
    totals = (total[0], total[1], sum_at_owner(branch_grads.astype(BF), "rep", 1)[0])
    velocities = (gate_velocity, up_velocity, branch_velocity)
    moments = [MOMENT * velocity + part for velocity, part in zip(velocities, totals)]
    gate, up, branch = [moment.astype(BF) for moment in moments]
    rows = gate.shape[0]
    width = gate.shape[1]
    place = lax.axis_index("tp")
    odd = place % 2

    wide = lax.all_gather(jnp.concatenate((gate, up), axis=0), "tp", axis=1, tiled=True)
    gate_wide, up_wide = wide[:rows], wide[rows:]
    branch_wide = lax.all_gather(branch, "tp", axis=1, tiled=True)
    turn = (((0,), (0,)), ((), ()))
    parts = [
        lax.dot_general(whole, own, turn, preferred_element_type=jnp.float32).astype(BF)
        for whole, own in ((gate_wide, gate), (up_wide, up), (branch_wide, branch))
    ]
    share = sum_at_owner(jnp.concatenate(parts[:2], axis=1), FS_REP, 0).astype(BF)
    share_b = sum_at_owner(parts[2], FS_REP, 0).astype(BF)
    swapped = lax.all_gather(share, "tp", axis=0, tiled=False)
    mine = jnp.where(odd == 0, swapped[:, :, :width], swapped[:, :, width:])
    mine = jnp.moveaxis(mine, 0, 1).reshape(mine.shape[1], -1)
    raw = lax.all_gather(mine, FS_REP, axis=0, tiled=True)
    line_b = lax.all_gather(share_b, "tp", axis=1, tiled=True)
    raw_b = lax.all_gather(line_b, FS_REP, axis=0, tiled=True)
    start = jnp.where(odd == 0, gate_wide, up_wide)

    x, m = chain(raw, start)
    xb, mb = chain(raw_b, branch_wide)
    final_b = last(xb, mb, place, branch.shape[1])
    half = rows // 2
    own = last(x, m, place, width)
    ahead = last(x[:half], m, (place + 1) % 4, width)
    behind = last(x[half:], m, (place + 3) % 4, width)
    low = lax.ppermute(ahead, "tp", [(i, (i + 1) % 4) for i in range(4)])
    high = lax.ppermute(behind, "tp", [(i, (i + 3) % 4) for i in range(4)])
    other = jnp.concatenate((low, high), axis=0)
    finals = (jnp.where(odd == 0, own, other), jnp.where(odd == 0, other, own), final_b)
    weights = (gate_weight, up_weight, branch_weight)
    heights = (FF, FF, D)
    results = []
    for moment, weight, final, height in zip(moments, weights, finals, heights):
        results.append(moment)
        results.append(SHRINK * weight - RATE * math.sqrt(height) * final.astype(jnp.float32))
    return tuple(results)


def solution(mesh):
    torus = Mesh(
        mesh.devices.reshape(4, 4, mesh.shape["tp"], mesh.shape["rep"]),
        ("fs_0", "fs_1", "tp", "rep"),
    )
    grads, plain = P("rep", FS, "tp"), P(FS_REP, "tp")
    return jax.shard_map(
        local,
        mesh=torus,
        in_specs=(grads, plain, plain) * 3,
        out_specs=(plain,) * 6,
        check_vma=False,
    )
```

time: 695 us -> 390 us (0.56)
  blocking collectives: 356 us -> 40.6 us
  matrix products: 37.3 us -> 193 us
  waiting for transfers between devices: 176 us -> 75 us
  starting transfers between devices: 67.3 us -> 22.3 us
    all_to_all x15 -> x2, blocking collectives: 254 us -> 9.27 us  [sum_at_owner(): tiles = lax.all_to_all(tiles, axis, 0, 0, tiled=True)]
    dot_general x27 -> x25, matrix products: 37.3 us -> 193 us  [the longest x22 188 us: dot(): return jnp.dot(a, b, preferred_element_type=jnp.float32)]
    all_to_all x14 -> x2, waiting for transfers between devices: 138 us -> 40.6 us  [sum_at_owner(): tiles = lax.all_to_all(tiles, axis, 0, 0, tiled=True)]
    all_to_all x14 -> x2, starting transfers between devices: 67 us -> 19.4 us  [sum_at_owner(): tiles = lax.all_to_all(tiles, axis, 0, 0, tiled=True)]
    all_gather x3, blocking collectives: 69.1 us -> 31.4 us  [the longest x1 10.9 us: local(): swapped = lax.all_gather(share, 'tp', axis=0, tiled=False)]
    psum x4 -> x0, blocking collectives: 32.6 us -> none  [by_axis(): value = lax.psum(value, axis)]
    broadcast_in_dim x18 -> x0, local copies, waits for them, and re-layouts: 7.06 us -> none  [from_everyone(): jnp.broadcast_to(value[None], (devices, *value.shape))]
    all_gather x6 -> x3, waiting for transfers between devices: 37.9 us -> 32.2 us  [the longest x1 27.3 us: local(): raw = lax.all_gather(mine, FS_REP, axis=0, tiled=True)]
  transfers between devices with their start and end apart: 20 -> 7, of which waited for: 14 -> 6; matrix products, arithmetic and copies ran while one was open for 8% -> 12% of each run, Pallas kernels for 0% -> 0%
where the time goes in v1:
time: 390 us; the launch traced here: 384 us
  matrix products  193 us (49%)
  waiting for transfers between devices  75 us (19%)
  blocking collectives  40.6 us (10%)
  other arithmetic  22.4 us (6%)
  starting transfers between devices  22.3 us (6%)
  between operations  18.9 us (5%)
  local copies, waits for them, and re-layouts  12.1 us (3%)
    dot_general x22, matrix products, dot(): return jnp.dot(a, b, preferred_element_type=jnp.float32)  188 us
    all_to_all x2, waiting for transfers between devices, sum_at_owner(): tiles = lax.all_to_all(tiles, axis, 0, 0, tiled=True)  40.6 us
    all_gather x1, waiting for transfers between devices, local(): raw = lax.all_gather(mine, FS_REP, axis=0, tiled=True)  27.3 us
    all_to_all x2, starting transfers between devices, sum_at_owner(): tiles = lax.all_to_all(tiles, axis, 0, 0, tiled=True)  19.4 us
    reduce_sum x2, other arithmetic, chain(): ratio = SAFETY * (jnp.sum(raw * raw) + 1.0) / (jnp.trace(raw) + 1.0)  11.6 us
    all_gather x1, blocking collectives, local(): swapped = lax.all_gather(share, 'tp', axis=0, tiled=False)  10.9 us
    all_gather x1, blocking collectives, local(): line_b = lax.all_gather(share_b, 'tp', axis=1, tiled=True)  10.6 us
    all_gather x1, blocking collectives, local(): branch_wide = lax.all_gather(branch, 'tp', axis=1, tiled=True)  9.89 us
  transfers between devices with their start and end apart: 7, of which 6 were waited for; matrix products, arithmetic and copies ran while one was open for 12% of the time, Pallas kernels for 0%

profile of v1, /device:TPU:1, one launch (start us, length us, event | category | flops | bytes accessed | tf_op | source)
XLA Modules:
  0.0 384.3 jit_solution(2413737595708279285)
XLA Ops:
  10.6 5.5 %all_to_all.20 = bf16[2,2,176,512]{3,2,1,0:T(8,128)(2,1)S(1)} all-to-all(bf16[2,2,176,512]{3,2,1,0:T(8,128)(2,1)S(1)} %copy.19), channel_id=1, replica_groups=mesh['fs_0'=4,'fs_1'=4,'tp'=4,'rep'=2] {'rep'}, dimensions={0} | all-to-all | bytes 1441792 | tf_op jit(solution)/shard_map/all_to_all | solution.py:32
  18.0 3.8 all_to_all.21
  22.5 9.9 %all_gather.25 = bf16[64,1024]{1,0:T(8,128)(2,1)S(1)} all-gather(bf16[64,256]{1,0:T(8,128)(2,1)S(1)} %get-tuple-element.10), channel_id=1, replica_groups=mesh['fs_0'=4,'fs_1'=4,'tp'=4,'rep'=2] {'tp'}, dimensions={1}, use_global_device_ids=true | all-gather | bytes 163840 | tf_op jit(solution)/shard_map/all_gather | solution.py:83
  33.6 11.5 %all-to-all-start.3 = ((bf16[32,32,256]{2,1,0:T(8,128)(2,1)}), bf16[32,32,256]{2,1,0:T(8,128)(2,1)S(1)}, u32[]{:S(2)}, u32[]{:S(2)}) async-start(bf16[32,32,256]{2,1,0:T(8,128)(2,1)} %bitcast.8), calls=%async_computation.3 | async-start | bytes 1048576 | tf_op jit(solution)/shard_map/all_to_all | solution.py:32
  49.4 2.6 pad_maximum_fusion
  52.0 6.4 %copy.20 = bf16[2048,1024]{1,0:T(8,128)(2,1)} copy(bf16[2048,1024]{0,1:T(8,128)(2,1)} %pad_maximum_fusion) | data formatting | bytes 8388608 | tf_op jit(solution)/shard_map/concatenate | solution.py:89
  58.4 7.9 %all-to-all-start.1 = ((bf16[32,64,1024]{2,1,0:T(8,128)(2,1)}), bf16[32,64,1024]{2,1,0:T(8,128)(2,1)}, u32[]{:S(2)}, u32[]{:S(2)}) async-start(bf16[32,64,1024]{2,1,0:T(8,128)(2,1)} %bitcast.56), calls=%async_computation.1 | async-start | bytes 8388608 | tf_op jit(solution)/shard_map/all_to_all | solution.py:32
  66.5 10.6 %all_gather.26 = bf16[32,1024]{1,0:T(8,128)(2,1)} all-gather(bf16[32,256]{1,0:T(8,128)(2,1)S(1)} %reduce_sum.85), channel_id=1, replica_groups=mesh['fs_0'=4,'fs_1'=4,'tp'=4,'rep'=2] {'tp'}, dimensions={1}, use_global_device_ids=true | all-gather | bytes 81920 | tf_op jit(solution)/shard_map/all_gather | solution.py:95
  77.2 40.6 %all-to-all-done.1 = bf16[32,64,1024]{2,1,0:T(8,128)(2,1)} async-done(((bf16[32,64,1024]{2,1,0:T(8,128)(2,1)}), bf16[32,64,1024]{2,1,0:T(8,128)(2,1)}, u32[]{:S(2)}, u32[]{:S(2)}) %all-to-all-start.1) | async-done | bytes 4194336 | tf_op jit(solution)/shard_map/all_to_all | solution.py:32
  117.7 3.1 reduce_sum.81
  120.9 10.9 %all-gather = bf16[256,1024]{1,0:T(8,128)(2,1)S(1)} all-gather(bf16[64,1024]{1,0:T(8,128)(2,1)S(1)} %reduce_sum.81), channel_id=2, replica_groups=mesh['fs_0'=4,'fs_1'=4,'tp'=4,'rep'=2] {'tp'}, dimensions={0}, use_global_device_ids=true | all-gather | bytes 655360 | tf_op jit(solution)/shard_map/all_gather | solution.py:91
  132.6 4.2 %all-gather.9.cloned.1.call-done = bf16[1024,1024]{1,0:T(8,128)(2,1)} async-done(((bf16[32,1024]{1,0:T(8,128)(2,1)}), bf16[1024,1024]{1,0:T(8,128)(2,1)}) %all-gather.9.cloned.1.call-update) | async-done | bytes 2097168 | tf_op jit(solution)/shard_map/all_gather | solution.py:96
  136.8 3.3 fusion.20
  141.5 5.6 %fusion.12 = bf16[1024,1024]{1,0:T(8,128)(2,1)S(1)} fusion(f32[]{:T(128)S(6)} %div.21, bf16[1024,1024]{1,0:T(8,128)(2,1)} %all-gather.9.cloned.1.call-done), kind=kOutput, calls=%fused_computation.30 | convolution fusion | flops 2159017984 | bytes 4194308 | tf_op jit(solution)/shard_map/dot_general | solution.py:25
  147.6 2.3 fusion.83
  150.0 2.7 add_convert_fusion.4
  152.7 2.5 fusion.16
  155.6 2.3 fusion.93
  158.0 3.0 add_convert_fusion.3
  161.0 2.3 fusion.94
  164.3 27.3 %all-gather.7.cloned.1.call-done = bf16[2048,2048]{1,0:T(8,128)(2,1)} async-done(((bf16[64,2048]{1,0:T(8,128)(2,1)}), bf16[2048,2048]{1,0:T(8,128)(2,1)}) %all-gather.7.cloned.1.call-update) | async-done | bytes 8388624 | tf_op jit(solution)/shard_map/all_gather | solution.py:94
  191.6 8.3 %fusion.9 = (f32[]{:T(128)}, f32[]{:T(128)}) fusion(bf16[2048,2048]{1,0:T(8,128)(2,1)} %all-gather.7.cloned.1.call-done), kind=kLoop, calls=%fused_computation.16 | loop fusion | flops 25165824 | bytes 8388616 | tf_op jit(solution)/shard_map/jit(trace)/reduce_sum | solution.py:38
  201.3 26.7 %fusion.1 = bf16[2048,2048]{1,0:T(8,128)(2,1)} fusion(f32[]{:T(128)S(6)} %div.18, bf16[2048,2048]{1,0:T(8,128)(2,1)} %all-gather.7.cloned.1.call-done), kind=kOutput, calls=%fused_computation.8 | convolution fusion | flops 17226006528 | bytes 16777220 | tf_op jit(solution)/shard_map/dot_general | solution.py:25
  228.0 22.7 %fusion.3 = bf16[2048,2048]{1,0:T(8,128)(2,1)} fusion(bf16[2048,2048]{1,0:T(8,128)(2,1)} %fusion.1, f32[]{:T(128)S(6)} %div.18, bf16[2048,2048]{1,0:T(8,128)(2,1)S(1)} %copy-done), kind=kOutput, calls=%fused_computation.10 | convolution fusion | flops 17221812224 | bytes 25165828 | tf_op jit(solution)/shard_map/dot_general | solution.py:25
  250.7 23.4 %add_convert_fusion.2 = bf16[2048,2048]{1,0:T(8,128)(2,1)S(1)} fusion(bf16[2048,2048]{1,0:T(8,128)(2,1)} %fusion.3, bf16[2048,2048]{1,0:T(8,128)(2,1)} %fusion.1), kind=kOutput, calls=%fused_computation.20 | convolution fusion | flops 17196646400 | bytes 25165824 | tf_op jit(solution)/shard_map/dot_general | solution.py:25
  274.1 3.2 copy-done.11
  277.3 18.7 %fusion.5 = bf16[2048,2048]{1,0:T(8,128)(2,1)S(1)} fusion(bf16[2048,2048]{1,0:T(8,128)(2,1)S(1)} %add_convert_fusion.2), kind=kOutput, calls=%fused_computation.12 | convolution fusion | flops 17200840704 | bytes 16777216 | tf_op jit(solution)/shard_map/dot_general | solution.py:25
  296.1 24.2 %fusion.7 = bf16[2048,2048]{1,0:T(8,128)(2,1)} fusion(bf16[2048,2048]{1,0:T(8,128)(2,1)} %copy-done.11, bf16[2048,2048]{1,0:T(8,128)(2,1)S(1)} %fusion.5), kind=kOutput, calls=%fused_computation.14 | convolution fusion | flops 17196646400 | bytes 25165824 | tf_op jit(solution)/shard_map/dot_general | solution.py:25
  320.3 1.9 fusion.23
  325.6 19.4 %add_convert_fusion.1 = bf16[2048,2048]{1,0:T(8,128)(2,1)} fusion(bf16[2048,2048]{1,0:T(8,128)(2,1)S(1)} %copy-done.10, bf16[2048,2048]{1,0:T(8,128)(2,1)S(1)} %fusion.5), kind=kOutput, calls=%fused_computation.19 | convolution fusion | flops 17196646400 | bytes 25165824 | tf_op jit(solution)/shard_map/dot_general | solution.py:25
  345.0 24.0 %add_convert_fusion = bf16[2048,2048]{1,0:T(8,128)(2,1)S(1)} fusion(bf16[2048,2048]{1,0:T(8,128)(2,1)} %add_convert_fusion.1), kind=kOutput, calls=%fused_computation.18 | convolution fusion | flops 17200840704 | bytes 16777216 | tf_op jit(solution)/shard_map/dot_general | solution.py:25
  372.9 1.9 collective-permute-done
  (65 shorter events, 22.6 us)
Async XLA Ops:
  8.0 8.2 %copy-start.3 = (f32[176,512]{1,0:T(8,128)S(1)}, f32[176,512]{1,0:T(8,128)}, u32[]{:S(2)}) copy-start(f32[176,512]{1,0:T(8,128)} %param.13) | copy-start | bytes 1081348
  8.0 8.2 %copy-start.4 = (f32[176,512]{1,0:T(8,128)S(1)}, f32[176,512]{1,0:T(8,128)}, u32[]{:S(2)}) copy-start(f32[176,512]{1,0:T(8,128)} %param.10) | copy-start | bytes 1081348
  8.0 37.7 %all-gather.5.cloned.1.call-start = ((), (), s32[]{:S(2)}) async-start(), calls=%async_computation.4 | async-start | bytes 1802240 | tf_op jit(solution)/shard_map/all_gather | solution.py:81
  10.5 7.5 %copy-start.7 = (f32[1,128,256]{2,1,0:T(8,128)S(1)}, f32[1,128,256]{2,1,0:T(8,128)}, u32[]{:S(2)}) copy-start(f32[1,128,256]{2,1,0:T(8,128)} %param.15) | copy-start | bytes 393220
  10.5 11.3 %copy-start.8 = (f32[64,256]{1,0:T(8,128)S(1)}, f32[64,256]{1,0:T(8,128)}, u32[]{:S(2)}) copy-start(f32[64,256]{1,0:T(8,128)} %param.16) | copy-start | bytes 196612
  33.6 24.9 %all-to-all-start.3 = ((bf16[32,32,256]{2,1,0:T(8,128)(2,1)}), bf16[32,32,256]{2,1,0:T(8,128)(2,1)S(1)}, u32[]{:S(2)}, u32[]{:S(2)}) async-start(bf16[32,32,256]{2,1,0:T(8,128)(2,1)} %bitcast.8), calls=%async_computation.3 | async-start | bytes 1048576 | tf_op jit(solution)/shard_map/all_to_all | solution.py:32
  58.4 59.3 %all-to-all-start.1 = ((bf16[32,64,1024]{2,1,0:T(8,128)(2,1)}), bf16[32,64,1024]{2,1,0:T(8,128)(2,1)}, u32[]{:S(2)}, u32[]{:S(2)}) async-start(bf16[32,64,1024]{2,1,0:T(8,128)(2,1)} %bitcast.56), calls=%async_computation.1 | async-start | bytes 8388608 | tf_op jit(solution)/shard_map/all_to_all | solution.py:32
  66.3 70.5 %all-gather.9.cloned.1.call-start = ((), (), s32[]{:S(2)}) async-start(), calls=%async_computation.6 | async-start | bytes 2162688 | tf_op jit(solution)/shard_map/all_gather | solution.py:96
  77.1 114.5 %all-gather.7.cloned.1.call-start = ((), (), s32[]{:S(2)}) async-start(), calls=%async_computation.5 | async-start | bytes 8650752 | tf_op jit(solution)/shard_map/all_gather | solution.py:94
  141.5 6.1 %copy-start.1 = (bf16[1024,1024]{1,0:T(8,128)(2,1)S(1)}, bf16[1024,1024]{1,0:T(8,128)(2,1)}, u32[]{:S(2)}) copy-start(bf16[1024,1024]{1,0:T(8,128)(2,1)} %all-gather.9.cloned.1.call-done) | copy-start | bytes 6291460
  161.0 2.4 copy-start.9
  201.3 26.7 %copy-start = (bf16[2048,2048]{1,0:T(8,128)(2,1)S(1)}, bf16[2048,2048]{1,0:T(8,128)(2,1)}, u32[]{:S(2)}) copy-start(bf16[2048,2048]{1,0:T(8,128)(2,1)} %all-gather.7.cloned.1.call-done) | copy-start | bytes 25165828
  274.1 3.2 copy-start.11
  277.3 42.9 %slice-start = ((s8[8388608]{0:T(1024)(128)(4,1)}), s8[4194304]{0:T(1024)(128)(4,1)S(1)}, s32[]{:S(2)}) async-start(s8[8388608]{0:T(1024)(128)(4,1)} %bitcast.61), calls=%async_computation.7 | async-start | bytes 8388608
  296.1 24.2 %copy-start.2 = (bf16[352,2048]{1,0:T(8,128)(2,1)S(1)}, bf16[352,2048]{1,0:T(8,128)(2,1)}, u32[]{:S(2)}) copy-start(bf16[352,2048]{1,0:T(8,128)(2,1)} %all-gather.5.cloned.1.call-done) | copy-start | bytes 4325380
  296.1 24.2 %slice-start.1 = ((s8[8388608]{0:T(1024)(128)(4,1)}), s8[4194304]{0:T(1024)(128)(4,1)S(1)}, s32[]{:S(2)}) async-start(s8[8388608]{0:T(1024)(128)(4,1)} %bitcast.61), calls=%async_computation.8 | async-start | bytes 8388608
  322.2 3.4 copy-start.10
  369.0 6.1 %copy-start.5 = (f32[176,512]{1,0:T(8,128)S(1)}, f32[176,512]{1,0:T(8,128)}, u32[]{:S(2)}) copy-start(f32[176,512]{1,0:T(8,128)} %param.14) | copy-start | bytes 1081348
  369.0 6.1 %copy-start.6 = (f32[176,512]{1,0:T(8,128)S(1)}, f32[176,512]{1,0:T(8,128)}, u32[]{:S(2)}) copy-start(f32[176,512]{1,0:T(8,128)} %param.11) | copy-start | bytes 1081348
  369.6 5.2 %collective-permute-start = (bf16[88,512]{1,0:T(8,128)(2,1)S(1)}, bf16[88,512]{1,0:T(8,128)(2,1)S(1)}, u32[]{:S(2)}, u32[]{:S(2)}) collective-permute-start(bf16[88,512]{1,0:T(8,128)(2,1)S(1)} %fusion.51), channel_id=1, source_target_pairs={{0,2},{2,4},{4,6},{6,0},{1,3},{3,5},{5,7},{7,1},{8,10},{10,12},{12... | collective-permute-start | bytes 270344 | tf_op jit(solution)/shard_map/ppermute | solution.py:106
  371.3 3.7 collective-permute-start.1
Sparse Core Ops, SparseCore 0:
  18.1 27.5 all-gather.4
Sparse Core Ops, SparseCore 1:
  77.2 59.6 all-gather.8
  139.5 52.0 all-gather.6

commit v2 on v1

--- a/solution.py
+++ b/solution.py
@@ -3,6 +3,8 @@
 import jax
 import jax.numpy as jnp
 from jax import lax
+from jax.experimental import pallas as pl
+from jax.experimental.pallas import tpu as pltpu
 from jax.sharding import Mesh
 from jax.sharding import PartitionSpec as P
 
@@ -31,6 +33,195 @@
     tiles = jnp.moveaxis(value.reshape(*before, devices, -1, *after), dim, 0)
     tiles = lax.all_to_all(tiles, axis, 0, 0, tiled=True)
     return jnp.sum(tiles.astype(jnp.float32), axis=0)
+
+
+N = 2048
+HALF = 1024
+CHUNK = 512
+STEPS = N // CHUNK
+
+
+def chunk_rows(r):
+    return pl.ds(pl.multiple_of(r * CHUNK, CHUNK), CHUNK)
+
+
+def iterate_kernel(
+    raw, x_in, w_gate, w_up, gate_out, up_out, a, b, c, m, x0, x1, x2, final, trace, load_sem, send, recv, xsend, xrecv, fsend, frecv
+):
+    core = lax.axis_index("rep")
+    place = lax.axis_index("tp")
+    other = 1 - core
+    kind = lax.rem(place, 2)
+    ahead = lax.rem(place + 1, 4)
+    behind = lax.rem(place + 3, 4)
+    rows = x_in.shape[0]
+    mine = pl.ds(pl.multiple_of(core * HALF, HALF), HALF)
+
+    loads = [pltpu.make_async_copy(raw.at[pl.ds(i * CHUNK, CHUNK)], a.at[pl.ds(i * CHUNK, CHUNK)], load_sem.at[i]) for i in range(STEPS)]
+    for copy in loads:
+        copy.start()
+
+    barrier = pltpu.get_barrier_semaphore()
+    pl.semaphore_signal(barrier, inc=1, device_id={"rep": other}, device_id_type=pl.DeviceIdType.MESH)
+    for near in (ahead, behind):
+        for to in range(2):
+            pl.semaphore_signal(barrier, inc=1, device_id={"tp": near, "rep": to}, device_id_type=pl.DeviceIdType.MESH)
+    pl.semaphore_wait(barrier, 5)
+
+    def remote(src, dst, ssem, rsem, to):
+        return pltpu.make_async_remote_copy(
+            src_ref=src, dst_ref=dst, send_sem=ssem, recv_sem=rsem, device_id=to, device_id_type=pl.DeviceIdType.MESH
+        )
+
+    partner = {"rep": other}
+
+    def swap(buf, k, r, half):
+        spot = buf.at[chunk_rows(r), pl.ds(pl.multiple_of(half * HALF, HALF), HALF)]
+        return remote(spot, spot, send.at[k, r], recv.at[k, r], partner)
+
+    def xswap(buf, k, half):
+        spot = buf.at[:, pl.ds(pl.multiple_of(half * HALF, HALF), HALF)]
+        return remote(spot, spot, xsend.at[k], xrecv.at[k], partner)
+
+    own_rows = pl.ds(pl.multiple_of(core * rows, 16), rows)
+    other_rows = pl.ds(pl.multiple_of(other * rows, 16), rows)
+    x0[own_rows] = x_in[...]
+    start_copy = remote(x0.at[own_rows], x0.at[own_rows], xsend.at[2], xrecv.at[2], partner)
+    start_copy.start()
+
+    for copy in loads:
+        copy.wait()
+
+    def squares(i, total):
+        part = a[pl.ds(pl.multiple_of(i * 64, 64), 64), :].astype(jnp.float32)
+        part = part * part
+        return total + jnp.sum(part.reshape(8, 8, N), axis=0)
+
+    second = jnp.sum(lax.fori_loop(0, N // 64, squares, jnp.zeros((8, N), jnp.float32)))
+    same = lax.broadcasted_iota(jnp.int32, (128, 128), 0) == lax.broadcasted_iota(jnp.int32, (128, 128), 1)
+    trace[...] = jnp.zeros((128, 128), jnp.float32)
+    for i in range(N // 128):
+        part = a[pl.ds(i * 128, 128), pl.ds(i * 128, 128)].astype(jnp.float32)
+        trace[...] += jnp.where(same, part, 0.0)
+    first = jnp.sum(trace[...])
+    second = jnp.full((1, 1), second)
+    first = jnp.full((1, 1), first)
+    ratio = SAFETY * (second + 1.0) / (first + 1.0)
+    alpha = 1.0 / ratio
+    scale = lax.rsqrt(ratio)
+
+    def square(left, k, low, high):
+        def step(r, _):
+            if k is not None:
+                swap(left, k, r, core).wait_send()
+                swap(left, k, r, other).wait_recv()
+            s = dot(left[chunk_rows(r), :], left[:, mine])
+            m[chunk_rows(r), :] = (low * left[chunk_rows(r), mine].astype(jnp.float32) + high * s).astype(BF)
+            return 0
+
+        lax.fori_loop(0, STEPS, step, 0)
+
+    def times(left, k, out, k_out, factor):
+        def step(r, _):
+            if k is not None:
+                swap(left, k, r, core).wait_send()
+                swap(left, k, r, other).wait_recv()
+            p = dot(left[chunk_rows(r), :], m[...])
+            p = COEF_ONE * left[chunk_rows(r), mine].astype(jnp.float32) + p
+            if factor is not None:
+                p = factor * p
+            out[chunk_rows(r), mine] = p.astype(BF)
+            swap(out, k_out, r, core).start()
+            return 0
+
+        lax.fori_loop(0, STEPS, step, 0)
+
+    square(a, None, COEF_THREE * alpha, COEF_FIVE * alpha * alpha)
+    times(a, None, b, 0, alpha)
+    start_copy.wait_send()
+    remote(x0.at[other_rows], x0.at[other_rows], xsend.at[2], xrecv.at[2], partner).wait_recv()
+    x1[:, mine] = (scale * (COEF_ONE * x0[:, mine].astype(jnp.float32) + dot(x0[...], m[...]))).astype(BF)
+    xswap(x1, 0, core).start()
+    times(b, 0, c, 1, None)
+    square(c, 1, COEF_THREE, COEF_FIVE)
+    times(c, None, b, 2, None)
+    xswap(x1, 0, core).wait_send()
+    xswap(x1, 0, other).wait_recv()
+    x2[:, mine] = (COEF_ONE * x1[:, mine].astype(jnp.float32) + dot(x1[...], m[...])).astype(BF)
+    xswap(x2, 1, core).start()
+    times(b, 2, a, 3, None)
+    square(a, 3, COEF_THREE, COEF_FIVE)
+    xswap(x2, 1, core).wait_send()
+    xswap(x2, 1, other).wait_recv()
+
+    def last(where, block):
+        cols = pl.ds(pl.multiple_of(block * 256, 256), 256)
+        near = pl.ds(pl.multiple_of(core * HALF + block * 256, 256), 256)
+        return (COEF_ONE * x2[where, near].astype(jnp.float32) + dot(x2[where, :], m[:, cols])).astype(BF)
+
+    lower, upper = pl.ds(0, rows), pl.ds(rows, rows)
+    final[2] = last(lower, ahead)
+    to_ahead = remote(final.at[2], final.at[4 + core], fsend.at[0], frecv.at[core], {"tp": ahead, "rep": 0})
+    to_ahead.start()
+    final[3] = last(upper, behind)
+    to_behind = remote(final.at[3], final.at[4 + core], fsend.at[1], frecv.at[core], {"tp": behind, "rep": 1})
+    to_behind.start()
+    final[6] = last(other_rows, place)
+    to_partner = remote(final.at[6], final.at[core], fsend.at[2], frecv.at[2], partner)
+    to_partner.start()
+    final[core] = last(own_rows, place)
+    to_ahead.wait_send()
+    to_behind.wait_send()
+    to_partner.wait_send()
+    remote(final.at[6], final.at[other], fsend.at[2], frecv.at[2], partner).wait_recv()
+    for i in range(2):
+        remote(final.at[2], final.at[4 + i], fsend.at[0], frecv.at[i], partner).wait_recv()
+    size = RATE * math.sqrt(FF)
+    for i in range(2):
+        cols = pl.ds(i * 256, 256)
+        owned = final[i].astype(jnp.float32)
+        fetched = final[4 + i].astype(jnp.float32)
+        even = kind == 0
+        gate_out[:, cols] = SHRINK * w_gate[:, cols] - size * jnp.where(even, owned, fetched)
+        up_out[:, cols] = SHRINK * w_up[:, cols] - size * jnp.where(even, fetched, owned)
+
+
+def iterate(raw, start, w_gate, w_up):
+    rows, width = w_gate.shape
+    whole = pl.BlockSpec(memory_space=pltpu.VMEM)
+    dma = pltpu.SemaphoreType.DMA
+    square = pltpu.VMEM((N, N), BF)
+    wide = pltpu.VMEM((2 * rows, N), BF)
+    return pl.pallas_call(
+        iterate_kernel,
+        out_shape=[jax.ShapeDtypeStruct((rows, width), jnp.float32)] * 2,
+        in_specs=[pl.BlockSpec(memory_space=pl.ANY), whole, whole, whole],
+        out_specs=[whole] * 2,
+        scratch_shapes=[
+            square,
+            square,
+            square,
+            pltpu.VMEM((N, HALF), BF),
+            wide,
+            wide,
+            wide,
+            pltpu.VMEM((7, rows, 256), BF),
+            pltpu.VMEM((128, 128), jnp.float32),
+            dma((STEPS,)),
+            dma((4, STEPS)),
+            dma((4, STEPS)),
+            dma((3,)),
+            dma((3,)),
+            dma((3,)),
+            dma((3,)),
+        ],
+        compiler_params=pltpu.CompilerParams(collective_id=0, has_side_effects=True, vmem_limit_bytes=60 * 1024 * 1024),
+    )(raw, start, w_gate, w_up)
+
+
+def inner_order(value):
+    rows = value.shape[0]
+    return jnp.swapaxes(value.reshape(rows, 4, 2, 256), 1, 2).reshape(rows, N)
 
 
 def chain(raw, start):
@@ -96,24 +287,12 @@
     raw_b = lax.all_gather(line_b, FS_REP, axis=0, tiled=True)
     start = jnp.where(odd == 0, gate_wide, up_wide)
 
-    x, m = chain(raw, start)
+    raw = inner_order(inner_order(raw).T)
+    gate_new, up_new = iterate(raw, inner_order(start), gate_weight, up_weight)
     xb, mb = chain(raw_b, branch_wide)
     final_b = last(xb, mb, place, branch.shape[1])
-    half = rows // 2
-    own = last(x, m, place, width)
-    ahead = last(x[:half], m, (place + 1) % 4, width)
-    behind = last(x[half:], m, (place + 3) % 4, width)
-    low = lax.ppermute(ahead, "tp", [(i, (i + 1) % 4) for i in range(4)])
-    high = lax.ppermute(behind, "tp", [(i, (i + 3) % 4) for i in range(4)])
-    other = jnp.concatenate((low, high), axis=0)
-    finals = (jnp.where(odd == 0, own, other), jnp.where(odd == 0, other, own), final_b)
-    weights = (gate_weight, up_weight, branch_weight)
-    heights = (FF, FF, D)
-    results = []
-    for moment, weight, final, height in zip(moments, weights, finals, heights):
-        results.append(moment)
-        results.append(SHRINK * weight - RATE * math.sqrt(height) * final.astype(jnp.float32))
-    return tuple(results)
+    branch_new = SHRINK * branch_weight - RATE * math.sqrt(D) * final_b.astype(jnp.float32)
+    return moments[0], gate_new, moments[1], up_new, moments[2], branch_new
 
 
 def solution(mesh):

time: 390 us -> 372 us (0.954)
  matrix products: 193 us -> 27.3 us
  Pallas kernels: 0 us -> 82.5 us
  local copies, waits for them, and re-layouts: 12.1 us -> 89.9 us
  other arithmetic: 22.4 us -> 14.2 us
    dot_general x22 -> x10, matrix products: 188 us -> 22.5 us  [dot(): return jnp.dot(a, b, preferred_element_type=jnp.float32)]
    pallas_call x0 -> x1, Pallas kernels: none -> 82.5 us  [iterate(): pl.pallas_call(iterate_kernel, out_shape=[jax.ShapeDtypeStruct((rows, wid...]
    reshape x0 -> x6, local copies, waits for them, and re-layouts: none -> 52.4 us  [inner_order(): return jnp.swapaxes(value.reshape(rows, 4, 2, 256), 1, 2).reshape(rows, N)]
    transpose x0 -> x2, local copies, waits for them, and re-layouts: none -> 26.8 us  [the longest x1 14.6 us: inner_order(): return jnp.swapaxes(value.reshape(rows, 4, 2, 256), 1, 2).reshape(rows, N)]
    reduce_sum x2 -> x1, other arithmetic: 11.6 us -> 3.3 us  [chain(): ratio = SAFETY * (jnp.sum(raw * raw) + 1.0) / (jnp.trace(raw) + 1.0)]
  transfers between devices with their start and end apart: 7 -> 5, of which waited for: 6 -> 4; matrix products, arithmetic and copies ran while one was open for 12% -> 13% of each run, Pallas kernels for 0% -> 0%
where the time goes in v2:
time: 372 us; the launch traced here: 365 us
  local copies, waits for them, and re-layouts  89.9 us (24%)
  Pallas kernels  82.5 us (22%)
  waiting for transfers between devices  74 us (20%)
  blocking collectives  40 us (11%)
  matrix products  27.3 us (7%)
  starting transfers between devices  19.5 us (5%)
  between operations  17.6 us (5%)
  other arithmetic  14.2 us (4%)
    pallas_call x1, Pallas kernels, iterate(): pl.pallas_call(iterate_kernel, out_shape=[jax.ShapeDtypeStruct((rows, wid...  82.5 us
    reshape x6, local copies, waits for them, and re-layouts, inner_order(): return jnp.swapaxes(value.reshape(rows, 4, 2, 256), 1, 2).reshape(rows, N)  52.4 us
    all_to_all x2, waiting for transfers between devices, sum_at_owner(): tiles = lax.all_to_all(tiles, axis, 0, 0, tiled=True)  40.4 us
    all_gather x1, waiting for transfers between devices, local(): raw = lax.all_gather(mine, FS_REP, axis=0, tiled=True)  27.5 us
    dot_general x10, matrix products, dot(): return jnp.dot(a, b, preferred_element_type=jnp.float32)  22.5 us
    all_to_all x2, starting transfers between devices, sum_at_owner(): tiles = lax.all_to_all(tiles, axis, 0, 0, tiled=True)  19.4 us
    transpose x1, local copies, waits for them, and re-layouts, inner_order(): return jnp.swapaxes(value.reshape(rows, 4, 2, 256), 1, 2).reshape(rows, N)  14.6 us
    transpose x1, local copies, waits for them, and re-layouts, local(): raw = inner_order(inner_order(raw).T)  12.2 us
  transfers between devices with their start and end apart: 5, of which 4 were waited for; matrix products, arithmetic and copies ran while one was open for 13% of the time, Pallas kernels for 0%

profile of v2, /device:TPU:1, one launch (start us, length us, event | category | flops | bytes accessed | tf_op | source)
XLA Modules:
  0.0 365.1 jit_solution(17683844524221162815)
XLA Ops:
  10.6 5.5 %all_to_all.20 = bf16[2,2,176,512]{3,2,1,0:T(8,128)(2,1)S(1)} all-to-all(bf16[2,2,176,512]{3,2,1,0:T(8,128)(2,1)S(1)} %copy.33), channel_id=1, replica_groups=mesh['fs_0'=4,'fs_1'=4,'tp'=4,'rep'=2] {'rep'}, dimensions={0} | all-to-all | bytes 1441792 | tf_op jit(solution)/shard_map/all_to_all | solution.py:34
  18.0 3.8 %all_to_all.21 = bf16[2,1,64,256]{3,2,1,0:T(8,128)(2,1)S(1)} all-to-all(bf16[2,1,64,256]{3,2,1,0:T(8,128)(2,1)S(1)} %bitcast.57), channel_id=1, replica_groups=mesh['fs_0'=4,'fs_1'=4,'tp'=4,'rep'=2] {'rep'}, dimensions={0} | all-to-all | bytes 131072 | tf_op jit(solution)/shard_map/all_to_all | solution.py:34
  22.5 9.9 %all_gather.25 = bf16[64,1024]{1,0:T(8,128)(2,1)S(1)} all-gather(bf16[64,256]{1,0:T(8,128)(2,1)S(1)} %get-tuple-element.12), channel_id=1, replica_groups=mesh['fs_0'=4,'fs_1'=4,'tp'=4,'rep'=2] {'tp'}, dimensions={1}, use_global_device_ids=true | all-gather | bytes 163840 | tf_op jit(solution)/shard_map/all_gather | solution.py:274
  33.6 11.5 %all-to-all-start.3 = ((bf16[32,32,256]{2,1,0:T(8,128)(2,1)}), bf16[32,32,256]{2,1,0:T(8,128)(2,1)S(1)}, u32[]{:S(2)}, u32[]{:S(2)}) async-start(bf16[32,32,256]{2,1,0:T(8,128)(2,1)} %bitcast.14), calls=%async_computation.3 | async-start | bytes 1048576 | tf_op jit(solution)/shard_map/all_to_all | solution.py:34
  45.7 1.9 convolution_convert_fusion
  47.6 1.9 convolution_convert_fusion.1
  49.4 2.6 pad_maximum_fusion
  52.0 6.4 %copy.34 = bf16[2048,1024]{1,0:T(8,128)(2,1)} copy(bf16[2048,1024]{0,1:T(8,128)(2,1)} %pad_maximum_fusion) | data formatting | bytes 8388608 | tf_op jit(solution)/shard_map/concatenate | solution.py:280
  58.4 7.9 %all-to-all-start.1 = ((bf16[32,64,1024]{2,1,0:T(8,128)(2,1)}), bf16[32,64,1024]{2,1,0:T(8,128)(2,1)}, u32[]{:S(2)}, u32[]{:S(2)}) async-start(bf16[32,64,1024]{2,1,0:T(8,128)(2,1)} %bitcast.52), calls=%async_computation.1 | async-start | bytes 8388608 | tf_op jit(solution)/shard_map/all_to_all | solution.py:34
  66.5 10.7 %all_gather.26 = bf16[32,1024]{1,0:T(8,128)(2,1)} all-gather(bf16[32,256]{1,0:T(8,128)(2,1)S(1)} %reduce_sum.64), channel_id=1, replica_groups=mesh['fs_0'=4,'fs_1'=4,'tp'=4,'rep'=2] {'tp'}, dimensions={1}, use_global_device_ids=true | all-gather | bytes 81920 | tf_op jit(solution)/shard_map/all_gather | solution.py:286
  77.3 40.4 %all-to-all-done.1 = bf16[32,64,1024]{2,1,0:T(8,128)(2,1)} async-done(((bf16[32,64,1024]{2,1,0:T(8,128)(2,1)}), bf16[32,64,1024]{2,1,0:T(8,128)(2,1)}, u32[]{:S(2)}, u32[]{:S(2)}) %all-to-all-start.1) | async-done | bytes 4194336 | tf_op jit(solution)/shard_map/all_to_all | solution.py:34
  117.7 3.1 reduce_sum.62
  120.9 10.1 %all-gather = bf16[256,1024]{1,0:T(8,128)(2,1)S(1)} all-gather(bf16[64,1024]{1,0:T(8,128)(2,1)S(1)} %reduce_sum.62), channel_id=2, replica_groups=mesh['fs_0'=4,'fs_1'=4,'tp'=4,'rep'=2] {'tp'}, dimensions={0}, use_global_device_ids=true | all-gather | bytes 655360 | tf_op jit(solution)/shard_map/all_gather | solution.py:282
  132.7 1.4 reshape.52.x_in
  134.2 5.4 %all-gather.9.cloned.1.call-done = bf16[1024,1024]{1,0:T(8,128)(2,1)} async-done(((bf16[32,1024]{1,0:T(8,128)(2,1)}), bf16[1024,1024]{1,0:T(8,128)(2,1)}) %all-gather.9.cloned.1.call-update) | async-done | bytes 2097168 | tf_op jit(solution)/shard_map/all_gather | solution.py:287
  139.5 3.3 fusion.9
  144.2 5.5 %fusion.1 = bf16[1024,1024]{1,0:T(8,128)(2,1)S(1)} fusion(f32[]{:T(128)S(6)} %div.9, bf16[1024,1024]{1,0:T(8,128)(2,1)} %all-gather.9.cloned.1.call-done), kind=kOutput, calls=%fused_computation.8 | convolution fusion | flops 2159017984 | bytes 4194308 | tf_op jit(solution)/shard_map/dot_general | solution.py:27
  150.3 2.3 fusion.36
  152.6 2.7 add_convert_fusion.1
  155.3 2.5 fusion.5
  158.3 2.6 fusion.45
  160.9 2.6 add_convert_fusion
  163.5 2.3 fusion.46
  166.8 27.5 %all-gather.7.cloned.1.call-done = bf16[2048,2048]{1,0:T(8,128)(2,1)} async-done(((bf16[64,2048]{1,0:T(8,128)(2,1)}), bf16[2048,2048]{1,0:T(8,128)(2,1)}) %all-gather.7.cloned.1.call-update) | async-done | bytes 8388624 | tf_op jit(solution)/shard_map/all_gather | solution.py:285
  194.3 14.5 %reshape.47 = bf16[2048,4,2,256]{3,2,1,0:T(2,128)(2,1)} reshape(bf16[2048,2048]{1,0:T(8,128)(2,1)} %all-gather.7.cloned.1.call-done) | data formatting | bytes 16777216 | tf_op jit(solution)/shard_map/reshape | solution.py:224
  208.8 21.2 %copy.36 = bf16[2048,4,2,256]{0,3,1,2:T(8,128)(2,1)} copy(bf16[2048,4,2,256]{3,2,1,0:T(2,128)(2,1)} %reshape.47) | data formatting | bytes 16777216 | tf_op jit(solution)/shard_map/reshape | solution.py:224
  230.0 12.2 %copy.37 = bf16[2048,2048]{0,1:T(8,128)(2,1)} copy(bf16[2048,2048]{1,0:T(8,128)(2,1)} %bitcast.50) | data formatting | bytes 16777216 | tf_op jit(solution)/shard_map/transpose | solution.py:290
  242.2 14.6 %copy.38 = bf16[2048,2,4,256]{3,2,1,0:T(4,128)(2,1)} copy(bf16[2048,2,4,256]{0,3,1,2:T(8,128)(2,1)} %bitcast.51) | data formatting | bytes 16777216 | tf_op jit(solution)/shard_map/transpose | solution.py:224
  256.8 14.4 %reshape.50.raw = bf16[2048,2048]{1,0:T(8,128)(2,1)} reshape(bf16[2048,2,4,256]{3,2,1,0:T(4,128)(2,1)} %copy.38) | data formatting | bytes 16777216 | tf_op jit(solution)/shard_map/reshape | solution.py:224
  271.2 82.5 %shard_map.136 = (f32[176,512]{1,0:T(8,128)}, f32[176,512]{1,0:T(8,128)}) custom-call(bf16[2048,2048]{1,0:T(8,128)(2,1)} %reshape.50.raw, bf16[176,2048]{1,0:T(8,128)(2,1)} %reshape.52.x_in, f32[176,512]{1,0:T(8,128)} %w_gate.1, f32[176,512]{1,0:T(8,128)} %w_up.1), custom_call_target="tpu_custom_call" | custom-call | tf_op jit(solution)/shard_map/pallas_call | solution.py:195
  353.7 1.7 copy.45
  355.4 1.7 copy.46
  (42 shorter events, 10.8 us)
Async XLA Ops:
  8.0 8.2 %copy-start.2 = (f32[176,512]{1,0:T(8,128)S(1)}, f32[176,512]{1,0:T(8,128)}, u32[]{:S(2)}) copy-start(f32[176,512]{1,0:T(8,128)} %param.13) | copy-start | bytes 1081348
  8.0 8.2 %copy-start.3 = (f32[176,512]{1,0:T(8,128)S(1)}, f32[176,512]{1,0:T(8,128)}, u32[]{:S(2)}) copy-start(f32[176,512]{1,0:T(8,128)} %param.10) | copy-start | bytes 1081348
  8.0 37.7 %all-gather.5.cloned.1.call-start = ((), (), s32[]{:S(2)}) async-start(), calls=%async_computation.4 | async-start | bytes 1802240 | tf_op jit(solution)/shard_map/all_gather | solution.py:272
  10.5 7.5 %copy-start.4 = (f32[1,128,256]{2,1,0:T(8,128)S(1)}, f32[1,128,256]{2,1,0:T(8,128)}, u32[]{:S(2)}) copy-start(f32[1,128,256]{2,1,0:T(8,128)} %param.15) | copy-start | bytes 393220
  10.5 11.3 %copy-start.5 = (f32[64,256]{1,0:T(8,128)S(1)}, f32[64,256]{1,0:T(8,128)}, u32[]{:S(2)}) copy-start(f32[64,256]{1,0:T(8,128)} %param.16) | copy-start | bytes 196612
  33.6 24.8 %all-to-all-start.3 = ((bf16[32,32,256]{2,1,0:T(8,128)(2,1)}), bf16[32,32,256]{2,1,0:T(8,128)(2,1)S(1)}, u32[]{:S(2)}, u32[]{:S(2)}) async-start(bf16[32,32,256]{2,1,0:T(8,128)(2,1)} %bitcast.14), calls=%async_computation.3 | async-start | bytes 1048576 | tf_op jit(solution)/shard_map/all_to_all | solution.py:34
  58.4 59.3 %all-to-all-start.1 = ((bf16[32,64,1024]{2,1,0:T(8,128)(2,1)}), bf16[32,64,1024]{2,1,0:T(8,128)(2,1)}, u32[]{:S(2)}, u32[]{:S(2)}) async-start(bf16[32,64,1024]{2,1,0:T(8,128)(2,1)} %bitcast.52), calls=%async_computation.1 | async-start | bytes 8388608 | tf_op jit(solution)/shard_map/all_to_all | solution.py:34
  66.3 65.4 %copy-start = (bf16[352,2048]{1,0:T(8,128)(2,1)S(1)}, bf16[352,2048]{1,0:T(8,128)(2,1)}, u32[]{:S(2)}) copy-start(bf16[352,2048]{1,0:T(8,128)(2,1)} %all-gather.5.cloned.1.call-done) | copy-start | bytes 4325380
  66.3 73.2 %all-gather.9.cloned.1.call-start = ((), (), s32[]{:S(2)}) async-start(), calls=%async_computation.6 | async-start | bytes 2162688 | tf_op jit(solution)/shard_map/all_gather | solution.py:287
  77.2 117.1 %all-gather.7.cloned.1.call-start = ((), (), s32[]{:S(2)}) async-start(), calls=%async_computation.5 | async-start | bytes 8650752 | tf_op jit(solution)/shard_map/all_gather | solution.py:285
  144.2 6.1 %copy-start.1 = (bf16[1024,1024]{1,0:T(8,128)(2,1)S(1)}, bf16[1024,1024]{1,0:T(8,128)(2,1)}, u32[]{:S(2)}) copy-start(bf16[1024,1024]{1,0:T(8,128)(2,1)} %all-gather.9.cloned.1.call-done) | copy-start | bytes 6291460
  163.5 2.4 copy-start.6
Sparse Core Ops, SparseCore 0:
  18.1 27.5 all-gather.4
Sparse Core Ops, SparseCore 1:
  77.3 62.2 all-gather.8
  142.2 52.0 all-gather.6

commit v3 on v1

v3 whole, which is shorter than its diff:
```python
import functools
import math

import jax
import jax.numpy as jnp
from jax import lax
from jax.experimental import pallas as pl
from jax.experimental.pallas import tpu as pltpu
from jax.sharding import Mesh
from jax.sharding import PartitionSpec as P

D = 2048
FF = 5632
FS_REP = ("fs_0", "fs_1", "rep")
FS = ("fs_0", "fs_1")

MOMENT = 0.95
COEF_ONE = 3.4445
COEF_THREE = -4.775
COEF_FIVE = 2.0315
SAFETY = 2.0
RATE = 0.5
SHRINK = 0.95
BF = jnp.bfloat16


def dot(a, b):
    return jnp.dot(a, b, preferred_element_type=jnp.float32)


N = 2048
HALF = 1024
CHUNK = 512
STEPS = N // CHUNK
NB = 1024
COPIES = 160
MESH = pl.DeviceIdType.MESH


def at(index, size):
    return pl.ds(index * size if isinstance(index, int) else pl.multiple_of(index * size, size), size)


def spot(offset, size, unit):
    return pl.ds(pl.multiple_of(offset, unit), size)


def turned(a, b):
    return lax.dot_general(a, b, (((0,), (0,)), ((), ())), preferred_element_type=jnp.float32)


def kernel(
    gate_g, up_g, branch_g, gate_v, up_v, branch_v, gate_w, up_w, branch_w,
    gate_m, gate_out, up_m, up_out, branch_m, branch_out,
    a, b, c, m, xs, xb, x1, x2, final,
    give, take, give_b, take_b,
    part, near, kept, near2, piece, panels,
    part_b, near_b, kept_b, near2_b, gram_b, m_b, t_b, g_b,
    sems, recvs, send, recv,
):
    core = lax.axis_index("rep")
    place = lax.axis_index("tp")
    iy = lax.axis_index("fs_1")
    iz = lax.axis_index("fs_0")
    other = 1 - core
    kind = lax.rem(place, 2)
    ahead = lax.rem(place + 1, 4)
    behind = lax.rem(place + 3, 4)
    across = lax.rem(place + 2, 4)
    rows = gate_v.shape[0]
    rows_b = branch_v.shape[0]
    mine = at(core, HALF)
    partner = {"rep": other}
    used = []

    def turn(axis, index, step):
        return {axis: lax.rem(index + step, 4)}

    def remote(src, dst, to):
        k = len(used)
        copy = pltpu.make_async_remote_copy(
            src_ref=src, dst_ref=dst, send_sem=sems.at[k], recv_sem=recvs.at[k], device_id=to, device_id_type=MESH
        )
        used.append(copy)
        return copy

    def send_to(ref, to):
        copy = remote(ref, ref, to)
        copy.start()
        return copy

    barrier = pltpu.get_barrier_semaphore()
    peers = [partner, {"tp": across}]
    peers += [{"tp": x, "rep": r} for x in (ahead, behind) for r in range(2)]
    peers += [turn(axis, index, step) for axis, index in (("fs_1", iy), ("fs_0", iz)) for step in (1, 2, 3)]
    for to in peers:
        pl.semaphore_signal(barrier, inc=1, device_id=to, device_id_type=MESH)

    own_rows, other_rows = at(core, rows), at(other, rows)
    give[0] = gate_g[0, other_rows, :].astype(BF)
    give[1] = up_g[0, other_rows, :].astype(BF)
    give_b[...] = branch_g[0, at(other, rows_b), :].astype(BF)
    pl.semaphore_wait(barrier, len(peers))
    first_copies = [remote(give_b, take_b, partner), remote(give, take, partner)]
    for copy in first_copies:
        copy.start()
    same = lax.broadcasted_iota(jnp.int32, (128, 128), 0) == lax.broadcasted_iota(jnp.int32, (128, 128), 1)

    def columns(ref, lines, height, width):
        def block(x, part):
            return ref.at[at(core, height), spot(part * 4 * width + x * width, width, width)]

        state = {}

        def start():
            state["right"] = [send_to(block(place, p), {"tp": ahead}) for p in range(2)]
            state["left"] = [send_to(block(place, p), {"tp": behind}) for p in range(2)]
            state["own"] = [send_to(block(place, p), partner) for p in range(2)]

        def second():
            state["right"][0].wait_recv()
            far = [send_to(block(behind, 0), {"tp": ahead})]
            state["left"][1].wait_recv()
            far.append(send_to(block(ahead, 1), {"tp": behind}))
            state["far"] = far
            state["own"].append(send_to(block(behind, 0), partner))
            state["own"].append(send_to(block(ahead, 1), partner))
            state["right"][1].wait_recv()
            state["own"].append(send_to(block(behind, 1), partner))
            state["left"][0].wait_recv()
            state["own"].append(send_to(block(ahead, 0), partner))

        def finish():
            for p in range(2):
                state["far"][p].wait_recv()
                state["own"].append(send_to(block(across, p), partner))
            for copy in state["own"]:
                copy.wait_recv()

        return start, second, finish

    gate_x, up_x = xs.at[0], xs.at[1]
    lines = [columns(xb, None, rows_b, 128), columns(gate_x, None, rows, 256), columns(up_x, None, rows, 256)]
    first_copies[0].wait_recv()
    moment = MOMENT * branch_v[...] + (branch_g[0, at(core, rows_b), :] + take_b[...].astype(jnp.float32))
    branch_m[...] = moment
    for p in range(2):
        xb[at(core, rows_b), spot(p * 512 + place * 128, 128, 128)] = moment[:, p * 128 : p * 128 + 128].astype(BF)
    lines[0][0]()
    first_copies[1].wait_recv()
    for i, (grads, velocity, out) in enumerate(((gate_g, gate_v, gate_m), (up_g, up_v, up_m))):
        moment = MOMENT * velocity[...] + (grads[0, own_rows, :] + take[i].astype(jnp.float32))
        out[...] = moment
        for p in range(2):
            xs[i, own_rows, spot(p * HALF + place * 256, 256, 256)] = moment[:, p * 256 : p * 256 + 256].astype(BF)
        lines[1 + i][0]()

    axes = ((("fs_1", iy), ("fs_0", iz)), (("fs_0", iz), ("fs_1", iy)))

    def exchange(source, landing, axis, index):
        copies = []
        for step in (2, 1, 3):
            to = lax.rem(index + step, 4)
            copies.append(remote(source(to), landing.at[step - 1], {axis: to}))
            copies[-1].start()
        return copies

    def total(own, landing, copies):
        for copy in copies:
            copy.wait_recv()
        value = own.astype(jnp.float32)
        for k in range(3):
            value = value + landing[k].astype(jnp.float32)
        return value.astype(BF)

    def scatter_one(source, landings):
        return [
            exchange(functools.partial(source, p), landings[p], *axes[p][0]) for p in range(2)
        ]

    def source_of(i):
        return lambda p, t: part.at[i, at(t, 64), at(p, 640)]

    def source_b(p, t):
        return part_b.at[spot(p * 64 + t * 16, 16, 16), :]

    lines[0][1]()
    lines[0][2]()
    part_b[...] = turned(xb[:, spot(core * 512 + place * 128, 128, 128)], xb[...]).astype(BF)
    one_b = scatter_one(source_b, [near_b.at[p] for p in range(2)])
    lines[1][1]()
    lines[2][1]()

    def panel(i):
        lines[1 + i][2]()
        own = xs[i, :, spot(core * HALF + place * 256, 256, 256)]
        for d in range(5):
            block = lax.rem(core * 4 + place + d, 8)
            part[i, :, at(d, 256)] = turned(own, xs[i, :, at(block, 256)]).astype(BF)
        return scatter_one(source_of(i), [near.at[i, p] for p in range(2)])

    ones = [panel(0)]
    two_b = []
    for p in range(2):
        kept_b[p] = total(part_b[spot(p * 64 + axes[p][0][1] * 16, 16, 16), :], near_b.at[p], one_b[p])
        two_b.append(exchange(lambda t, p=p: kept_b.at[p, :, at(t, 256)], near2_b.at[p], *axes[p][1]))
    ones.append(panel(1))

    def gram_rows(p, i1):
        return spot(p * 64 + i1 * 16, 16, 16)

    group = at(core, 4)
    swaps_b = []
    for p in range(2):
        i1, i2 = axes[p][0][1], axes[p][1][1]
        gram_b[core * 4 + place, gram_rows(p, i1), at(i2, 256)] = total(
            kept_b[p, :, at(i2, 256)], near2_b.at[p], two_b[p]
        )
        ref = gram_b.at[core * 4 + place, gram_rows(p, i1), at(i2, 256)]
        swaps_b.append([send_to(ref, {"tp": x}) for x in (across, ahead, behind)])
    twos = []
    for i in range(2):
        pair = []
        for p in range(2):
            index = axes[p][0][1]
            kept[i, p] = total(part[i, at(index, 64), at(p, 640)], near.at[i, p], ones[i][p])
            pair.append(exchange(lambda t, i=i, p=p: kept.at[i, p, at(t, 16), :], near2.at[i, p], *axes[p][1]))
        twos.append(pair)

    class Ring:
        def __init__(self, axis, index, block, cut):
            self.next, self.prev = turn(axis, index, 1), turn(axis, index, 3)
            self.index, self.block, self.cut = index, block, cut

        def start(self):
            ref = self.block(self.index)
            self.right = send_to(ref, self.next)
            self.left = send_to(ref, self.prev)

        def second(self):
            self.right.wait_recv()
            self.far = [send_to(self.cut(lax.rem(self.index + 3, 4), 0), self.next)]
            self.left.wait_recv()
            self.far.append(send_to(self.cut(lax.rem(self.index + 1, 4), 1), self.prev))

        def finish(self):
            for copy in self.far:
                copy.wait_recv()

    def rings(phase, block, cut):
        return [
            Ring(*axes[p][phase], functools.partial(block, p), functools.partial(cut, p)) for p in range(2)
        ]

    def b_small(p, j):
        return gram_b.at[group, gram_rows(p, axes[p][0][1]), at(j, 256)]

    def b_small_cut(p, j, h):
        return gram_b.at[at(core * 2 + h, 2), gram_rows(p, axes[p][0][1]), at(j, 256)]

    def b_large(p, j):
        return gram_b.at[group, gram_rows(p, j), :]

    def b_large_cut(p, j, h):
        return gram_b.at[at(core * 2 + h, 2), gram_rows(p, j), :]

    def g_rows(p, j):
        return spot(axes[p][0][1] * 64 + j * 16, 16, 16)

    def g_small(p, j):
        return panels.at[core, :, g_rows(p, j), at(p, 640)]

    def g_small_cut(p, j, h):
        return panels.at[core, at(h, 2), g_rows(p, j), at(p, 640)]

    def g_large(p, j):
        return panels.at[core, :, at(j, 64), at(p, 640)]

    def g_large_cut(p, j, h):
        return panels.at[core, at(h, 2), at(j, 64), at(p, 640)]

    small_b, large_b = rings(1, b_small, b_small_cut), rings(0, b_large, b_large_cut)
    small, large = rings(1, g_small, g_small_cut), rings(0, g_large, g_large_cut)
    for p in range(2):
        for copy in swaps_b[p]:
            copy.wait_recv()
        small_b[p].start()
    swaps = []
    for p in range(2):
        i2 = axes[p][1][1]
        for i in range(2):
            piece[i, p] = total(kept[i, p, at(i2, 16), :], near2.at[i, p], twos[i][p])
        target = panels.at[core, place, g_rows(p, i2), at(p, 640)]
        panels[core, place, g_rows(p, i2), at(p, 640)] = piece[kind, p]
        swaps.append(send_to(target, {"tp": across}))
        for x in (ahead, behind):
            copy = remote(piece.at[1 - kind, p], target, {"tp": x})
            copy.start()
            swaps.append(copy)
    for ring in small_b:
        ring.second()
    for copy in swaps:
        copy.wait_recv()
    for ring in small:
        ring.start()
    for ring in small_b:
        ring.finish()
    for ring in large_b:
        ring.start()
    for ring in small:
        ring.second()
    forward_b, forward = [], []
    for p, ring in enumerate(large_b):
        ring.second()
        forward_b += [send_to(b_large(p, lax.rem(ring.index + k, 4)), partner) for k in (0, 3, 1)]
    for ring in small:
        ring.finish()
    for ring in large:
        ring.start()
    for p, ring in enumerate(large_b):
        ring.finish()
        forward_b.append(send_to(b_large(p, lax.rem(ring.index + 2, 4)), partner))
    for copy in forward_b:
        copy.wait_recv()

    def coefficients(squares, diagonal):
        second = jnp.full((1, 1), squares)
        first = jnp.full((1, 1), diagonal)
        ratio = SAFETY * (second + 1.0) / (first + 1.0)
        return 1.0 / ratio, lax.rsqrt(ratio)

    def squares_b(i, sums):
        value = gram_b[i].astype(jnp.float32)
        diagonal = gram_b[i, :, at(i, 128)].astype(jnp.float32)
        return (
            sums[0] + jnp.sum((value * value).reshape(16, 8, NB), axis=0),
            sums[1] + jnp.where(same, diagonal, 0.0),
        )

    sums = lax.fori_loop(0, 8, squares_b, (jnp.zeros((8, NB), jnp.float32), jnp.zeros((128, 128), jnp.float32)))
    alpha_b, scale_b = coefficients(jnp.sum(sums[0]), jnp.sum(sums[1]))

    def square_b(left, low, high):
        def step(r, _):
            where = at(r, 512)
            m_b[where, :] = (low * left[where, :].astype(jnp.float32) + high * dot(left[where, :], left[...])).astype(BF)
            return 0

        lax.fori_loop(0, 2, step, 0)

    def times_b(left, out, factor):
        def step(r, _):
            where = at(r, 512)
            value = factor * (COEF_ONE * left[where, :].astype(jnp.float32) + dot(left[where, :], m_b[...]))
            out[where, :] = value.astype(BF)
            return 0

        lax.fori_loop(0, 2, step, 0)

    def rows_of(left, factor):
        return (factor * (COEF_ONE * left.astype(jnp.float32) + dot(left, m_b[...]))).astype(BF)

    for i in range(8):
        g_b[at(i, 128), :] = gram_b[i]
    square_b(g_b, COEF_THREE * alpha_b, COEF_FIVE * alpha_b * alpha_b)
    times_b(g_b, t_b, alpha_b)
    line = rows_of(xb[at(core, rows_b), :], scale_b)
    times_b(t_b, g_b, 1.0)
    square_b(g_b, COEF_THREE, COEF_FIVE)
    for p, ring in enumerate(large):
        ring.second()
        forward += [send_to(g_large(p, lax.rem(ring.index + k, 4)), partner) for k in (0, 3, 1)]
    times_b(g_b, t_b, 1.0)
    line = rows_of(line, 1.0)
    times_b(t_b, g_b, 1.0)
    for p, ring in enumerate(large):
        ring.finish()
        forward.append(send_to(g_large(p, lax.rem(ring.index + 2, 4)), partner))
    square_b(g_b, COEF_THREE, COEF_FIVE)
    t_b[0:rows_b, :] = line
    for p in range(2):
        cols = spot(p * 512 + place * 128, 128, 128)
        last_b = COEF_ONE * t_b[0:rows_b, cols].astype(jnp.float32) + dot(line, m_b[:, cols])
        branch_out[:, at(p, 128)] = SHRINK * branch_w[:, at(p, 128)] - RATE * math.sqrt(D) * last_b.astype(BF).astype(
            jnp.float32
        )
    for copy in forward:
        copy.wait_recv()

    def assemble(r, sums):
        value = panels[lax.div(r, 4), lax.rem(r, 4)]
        squares, diagonal = sums
        for d in range(5):
            block = value[:, d * 256 : d * 256 + 256]
            column = at(lax.rem(r + d, 8), 256)
            a[at(r, 256), column] = block
            if 0 < d < 4:
                a[column, at(r, 256)] = block.T
            wide = block.astype(jnp.float32)
            weight = 2.0 if 0 < d < 4 else 1.0
            squares = squares + weight * jnp.sum((wide * wide).reshape(32, 8, 256), axis=0)
        for k in range(2):
            corner = value[k * 128 : k * 128 + 128, k * 128 : k * 128 + 128].astype(jnp.float32)
            diagonal = diagonal + jnp.where(same, corner, 0.0)
        return squares, diagonal

    sums = lax.fori_loop(0, 8, assemble, (jnp.zeros((8, 256), jnp.float32), jnp.zeros((128, 128), jnp.float32)))
    alpha, scale = coefficients(jnp.sum(sums[0]), jnp.sum(sums[1]))

    x0 = xs.at[kind]

    def swap(buf, k, r, half):
        ref = buf.at[at(r, CHUNK), at(half, HALF)]
        return pltpu.make_async_remote_copy(
            src_ref=ref, dst_ref=ref, send_sem=send.at[k, r], recv_sem=recv.at[k, r], device_id=partner, device_id_type=MESH
        )

    def square(left, k, low, high):
        def step(r, _):
            if k is not None:
                swap(left, k, r, core).wait_send()
                swap(left, k, r, other).wait_recv()
            s = dot(left[at(r, CHUNK), :], left[:, mine])
            m[at(r, CHUNK), :] = (low * left[at(r, CHUNK), mine].astype(jnp.float32) + high * s).astype(BF)
            return 0

        lax.fori_loop(0, STEPS, step, 0)

    def times(left, k, out, k_out, factor):
        def step(r, _):
            if k is not None:
                swap(left, k, r, core).wait_send()
                swap(left, k, r, other).wait_recv()
            p = dot(left[at(r, CHUNK), :], m[...])
            p = COEF_ONE * left[at(r, CHUNK), mine].astype(jnp.float32) + p
            if factor is not None:
                p = factor * p
            out[at(r, CHUNK), mine] = p.astype(BF)
            swap(out, k_out, r, core).start()
            return 0

        lax.fori_loop(0, STEPS, step, 0)

    square(a, None, COEF_THREE * alpha, COEF_FIVE * alpha * alpha)
    times(a, None, b, 0, alpha)
    x1[:, mine] = (scale * (COEF_ONE * x0[:, mine].astype(jnp.float32) + dot(x0[...], m[...]))).astype(BF)
    turn_one = send_to(x1.at[:, mine], partner)
    times(b, 0, c, 1, None)
    square(c, 1, COEF_THREE, COEF_FIVE)
    times(c, None, b, 2, None)
    turn_one.wait_recv()
    x2[:, mine] = (COEF_ONE * x1[:, mine].astype(jnp.float32) + dot(x1[...], m[...])).astype(BF)
    turn_two = send_to(x2.at[:, mine], partner)
    times(b, 2, a, 3, None)
    square(a, 3, COEF_THREE, COEF_FIVE)
    turn_two.wait_recv()

    def last(where, block):
        cols = at(block, 256)
        close = spot(core * HALF + block * 256, 256, 256)
        return (COEF_ONE * x2[where, close].astype(jnp.float32) + dot(x2[where, :], m[:, cols])).astype(BF)

    final[2] = last(pl.ds(0, rows), ahead)
    to_ahead = pltpu.make_async_remote_copy(
        src_ref=final.at[2], dst_ref=final.at[4 + core], send_sem=sems.at[COPIES], recv_sem=recvs.at[COPIES + core],
        device_id={"tp": ahead, "rep": 0}, device_id_type=MESH,
    )
    to_ahead.start()
    final[3] = last(pl.ds(rows, rows), behind)
    to_behind = pltpu.make_async_remote_copy(
        src_ref=final.at[3], dst_ref=final.at[4 + core], send_sem=sems.at[COPIES + 1], recv_sem=recvs.at[COPIES + core],
        device_id={"tp": behind, "rep": 1}, device_id_type=MESH,
    )
    to_behind.start()
    final[6] = last(other_rows, place)
    to_partner = remote(final.at[6], final.at[core], partner)
    to_partner.start()
    final[core] = last(own_rows, place)
    to_partner.wait_recv()
    for i in range(2):
        pltpu.make_async_remote_copy(
            src_ref=final.at[2], dst_ref=final.at[4 + i], send_sem=sems.at[COPIES], recv_sem=recvs.at[COPIES + i],
            device_id=partner, device_id_type=MESH,
        ).wait_recv()
    size = RATE * math.sqrt(FF)
    for i in range(2):
        cols = pl.ds(i * 256, 256)
        owned = final[i].astype(jnp.float32)
        fetched = final[4 + i].astype(jnp.float32)
        even = kind == 0
        gate_out[:, cols] = SHRINK * gate_w[:, cols] - size * jnp.where(even, owned, fetched)
        up_out[:, cols] = SHRINK * up_w[:, cols] - size * jnp.where(even, fetched, owned)
    to_ahead.wait_send()
    to_behind.wait_send()
    for copy in used:
        copy.wait_send()


def local(*args):
    velocities = (args[1], args[4], args[7])
    rows, width = velocities[0].shape
    rows_b, width_b = velocities[2].shape
    whole = pl.BlockSpec(memory_space=pltpu.VMEM)
    dma = pltpu.SemaphoreType.DMA

    def buf(*shape):
        return pltpu.VMEM(shape, BF)

    outs = []
    for velocity in velocities:
        outs += [jax.ShapeDtypeStruct(velocity.shape, jnp.float32)] * 2
    return pl.pallas_call(
        kernel,
        out_shape=outs,
        in_specs=[whole] * 9,
        out_specs=[whole] * 6,
        scratch_shapes=[
            buf(N, N), buf(N, N), buf(N, N), buf(N, HALF),
            buf(2, 2 * rows, N), buf(2 * rows_b, NB), buf(2 * rows, N), buf(2 * rows, N), buf(7, rows, 256),
            buf(2, rows, width), buf(2, rows, width), buf(rows_b, width_b), buf(rows_b, width_b),
            buf(2, 256, 1280), buf(2, 2, 3, 64, 640), buf(2, 2, 64, 640), buf(2, 2, 3, 16, 640), buf(2, 2, 16, 640),
            buf(2, 4, 256, 1280),
            buf(128, NB), buf(2, 3, 16, NB), buf(2, 16, NB), buf(2, 3, 16, 256), buf(8, 128, NB),
            buf(NB, NB), buf(NB, NB), buf(NB, NB),
            dma((COPIES + 2,)), dma((COPIES + 2,)), dma((4, STEPS)), dma((4, STEPS)),
        ],
        compiler_params=pltpu.CompilerParams(collective_id=0, has_side_effects=True, vmem_limit_bytes=63 * 1024 * 1024),
    )(args[0], args[3], args[6], args[1], args[4], args[7], args[2], args[5], args[8])


def solution(mesh):
    torus = Mesh(
        mesh.devices.reshape(4, 4, mesh.shape["tp"], mesh.shape["rep"]),
        ("fs_0", "fs_1", "tp", "rep"),
    )
    grads, plain = P("rep", FS, "tp"), P(FS_REP, "tp")
    return jax.shard_map(
        local,
        mesh=torus,
        in_specs=(grads, plain, plain) * 3,
        out_specs=(plain,) * 6,
        check_vma=False,
    )
```

time: 390 us -> 168 us (0.43); the launches traced: 384 us -> 168 us
  matrix products: 193 us -> 0 us
  Pallas kernels: 0 us -> 161 us
  waiting for transfers between devices: 75 us -> 0 us
  blocking collectives: 40.6 us -> 0 us
  other arithmetic: 22.4 us -> 0 us
  starting transfers between devices: 22.3 us -> 0 us
  between operations: 18.9 us -> 0.66 us
  local copies, waits for them, and re-layouts: 12.1 us -> 6.38 us
    dot_general x25 -> x0, matrix products: 193 us -> none  [the longest x22 188 us: dot(): return jnp.dot(a, b, preferred_element_type=jnp.float32)]
    pallas_call x0 -> x1, Pallas kernels: none -> 161 us  [local(): pl.pallas_call(kernel, out_shape=outs, in_specs=[whole] * 9, out_specs=[w...]
    all_to_all x2 -> x0, waiting for transfers between devices: 40.6 us -> none  [sum_at_owner(): tiles = lax.all_to_all(tiles, axis, 0, 0, tiled=True)]
    all_gather x3 -> x0, waiting for transfers between devices: 32.2 us -> none  [the longest x1 27.3 us: local(): raw = lax.all_gather(mine, FS_REP, axis=0, tiled=True)]
    all_gather x3 -> x0, blocking collectives: 31.4 us -> none  [the longest x1 10.9 us: local(): swapped = lax.all_gather(share, 'tp', axis=0, tiled=False)]
    all_to_all x2 -> x0, starting transfers between devices: 19.4 us -> none  [sum_at_owner(): tiles = lax.all_to_all(tiles, axis, 0, 0, tiled=True)]
    reduce_sum x6 -> x0, other arithmetic: 15 us -> none  [the longest x2 11.6 us: chain(): ratio = SAFETY * (jnp.sum(raw * raw) + 1.0) / (jnp.trace(raw) + 1.0)]
    all_to_all x2 -> x0, blocking collectives: 9.27 us -> none  [sum_at_owner(): tiles = lax.all_to_all(tiles, axis, 0, 0, tiled=True)]
  transfers between devices with their start and end apart: 7 -> 0, of which waited for: 6 -> 0; matrix products, arithmetic and copies ran while one was open for 12% -> 0% of each run, Pallas kernels for 0% -> 0%
where the time goes in v3:
time: 168 us
  Pallas kernels  161 us (96%)
  local copies, waits for them, and re-layouts  6.38 us (4%)
    pallas_call x1, Pallas kernels, local(): pl.pallas_call(kernel, out_shape=outs, in_specs=[whole] * 9, out_specs=[w...  161 us
    unnamed x16, local copies, waits for them, and re-layouts  6.38 us

profile of v3, /device:TPU:1, one launch (start us, length us, event | category | flops | bytes accessed | tf_op | source)
XLA Modules:
  0.0 167.7 jit_solution(1695096314932797578)
XLA Ops:
  0.6 160.7 %shard_map.136 = (f32[176,512]{1,0:T(8,128)}, f32[176,512]{1,0:T(8,128)}, f32[176,512]{1,0:T(8,128)}, f32[176,512]{1,0:T(8,128)}, f32[64,256]{1,0:T(8,128)}, /*index=5*/f32[64,256]{1,0:T(8,128)}) custom-call(f32[1,352,512]{2,1,0:T(8,128)} %gate_g.1, f32[1,352,512]{2,1,0:T(8,128)} %up_g.1, f32[1,128,256]{2,1,0:T(8,128)} %branch_g.1, f32[176,512]{1,0:T(8,128)} %gate_v.1, ...), custom_call_target="tpu_custom_call" | custom-call | tf_op jit(solution)/shard_map/pallas_call | solution.py:512
  161.3 0.0 copy-start.2
  161.3 1.8 %copy.21 = f32[176,512]{1,0:T(8,128)} copy(f32[176,512]{1,0:T(8,128)} %get-tuple-element.12) | data formatting | bytes 720896
  163.1 0.0 copy-done.2
  163.1 0.0 copy-start.1
  163.1 0.7 copy.22
  163.9 0.4 copy-done.1
  164.3 0.0 copy-start
  164.3 0.7 copy.23
  165.0 0.4 copy-done
  165.4 0.0 copy-start.4
  165.4 0.7 copy.24
  166.1 0.1 copy-done.4
  166.2 0.0 copy-start.3
  166.2 0.6 copy.25
  166.9 0.2 copy-done.3
  167.1 0.6 copy.26
Async XLA Ops:
  161.3 1.8 %copy-start.2 = (f32[176,512]{1,0:T(8,128)S(1)}, f32[176,512]{1,0:T(8,128)}, u32[]{:S(2)}) copy-start(f32[176,512]{1,0:T(8,128)} %get-tuple-element.13) | copy-start | bytes 1081348
  163.1 1.1 copy-start.1
  164.3 1.1 copy-start
  165.4 0.9 copy-start.4
  166.2 0.9 copy-start.3

commit v4 on v3

--- a/solution.py
+++ b/solution.py
@@ -50,8 +50,9 @@
 
 
 def kernel(
-    gate_g, up_g, branch_g, gate_v, up_v, branch_v, gate_w, up_w, branch_w,
-    gate_m, gate_out, up_m, up_out, branch_m, branch_out,
+    gate_g, up_g, branch_g, gate_v, up_v, branch_v,
+    gate_m, up_m, branch_m, gate_out, up_out, branch_out,
+    grads, grads_b, speed, speed_b, results, results_b, in_sem, out_sem,
     a, b, c, m, xs, xb, x1, x2, final,
     give, take, give_b, take_b,
     part, near, kept, near2, piece, panels,
@@ -69,6 +70,22 @@
     across = lax.rem(place + 2, 4)
     rows = gate_v.shape[0]
     rows_b = branch_v.shape[0]
+    loads = []
+
+    def load(source, target):
+        copy = pltpu.make_async_copy(source, target, in_sem.at[len(loads)])
+        copy.start()
+        loads.append(copy)
+
+    load(branch_g.at[0, at(other, rows_b)], grads_b.at[1])
+    load(gate_g.at[0, at(other, rows)], grads.at[0, 1])
+    load(up_g.at[0, at(other, rows)], grads.at[1, 1])
+    load(branch_g.at[0, at(core, rows_b)], grads_b.at[0])
+    load(branch_v, speed_b)
+    load(gate_g.at[0, at(core, rows)], grads.at[0, 0])
+    load(gate_v, speed.at[0])
+    load(up_g.at[0, at(core, rows)], grads.at[1, 0])
+    load(up_v, speed.at[1])
     mine = at(core, HALF)
     partner = {"rep": other}
     used = []
@@ -97,11 +114,14 @@
         pl.semaphore_signal(barrier, inc=1, device_id=to, device_id_type=MESH)
 
     own_rows, other_rows = at(core, rows), at(other, rows)
-    give[0] = gate_g[0, other_rows, :].astype(BF)
-    give[1] = up_g[0, other_rows, :].astype(BF)
-    give_b[...] = branch_g[0, at(other, rows_b), :].astype(BF)
+    loads[0].wait()
+    give_b[...] = grads_b[1].astype(BF)
+    for i in range(2):
+        loads[1 + i].wait()
+        give[i] = grads[i, 1].astype(BF)
     pl.semaphore_wait(barrier, len(peers))
-    first_copies = [remote(give_b, take_b, partner), remote(give, take, partner)]
+    first_copies = [remote(give_b, take_b, partner)]
+    first_copies += [remote(give.at[i], take.at[i], partner) for i in range(2)]
     for copy in first_copies:
         copy.start()
     same = lax.broadcasted_iota(jnp.int32, (128, 128), 0) == lax.broadcasted_iota(jnp.int32, (128, 128), 1)
@@ -142,18 +162,28 @@
     gate_x, up_x = xs.at[0], xs.at[1]
     lines = [columns(xb, None, rows_b, 128), columns(gate_x, None, rows, 256), columns(up_x, None, rows, 256)]
     first_copies[0].wait_recv()
-    moment = MOMENT * branch_v[...] + (branch_g[0, at(core, rows_b), :] + take_b[...].astype(jnp.float32))
-    branch_m[...] = moment
+    loads[3].wait()
+    loads[4].wait()
+    moment = MOMENT * speed_b[...] + (grads_b[0] + take_b[...].astype(jnp.float32))
+    speed_b[...] = moment
     for p in range(2):
         xb[at(core, rows_b), spot(p * 512 + place * 128, 128, 128)] = moment[:, p * 128 : p * 128 + 128].astype(BF)
     lines[0][0]()
-    first_copies[1].wait_recv()
-    for i, (grads, velocity, out) in enumerate(((gate_g, gate_v, gate_m), (up_g, up_v, up_m))):
-        moment = MOMENT * velocity[...] + (grads[0, own_rows, :] + take[i].astype(jnp.float32))
-        out[...] = moment
+    for i in range(2):
+        first_copies[1 + i].wait_recv()
+        loads[5 + 2 * i].wait()
+        loads[6 + 2 * i].wait()
+        moment = MOMENT * speed[i] + (grads[i, 0] + take[i].astype(jnp.float32))
+        speed[i] = moment
         for p in range(2):
             xs[i, own_rows, spot(p * HALF + place * 256, 256, 256)] = moment[:, p * 256 : p * 256 + 256].astype(BF)
         lines[1 + i][0]()
+    stores = []
+
+    def store(source, target):
+        copy = pltpu.make_async_copy(source, target, out_sem.at[len(stores)])
+        copy.start()
+        stores.append(copy)
 
     axes = ((("fs_1", iy), ("fs_0", iz)), (("fs_0", iz), ("fs_1", iy)))
 
@@ -184,13 +214,6 @@
     def source_b(p, t):
         return part_b.at[spot(p * 64 + t * 16, 16, 16), :]
 
-    lines[0][1]()
-    lines[0][2]()
-    part_b[...] = turned(xb[:, spot(core * 512 + place * 128, 128, 128)], xb[...]).astype(BF)
-    one_b = scatter_one(source_b, [near_b.at[p] for p in range(2)])
-    lines[1][1]()
-    lines[2][1]()
-
     def panel(i):
         lines[1 + i][2]()
         own = xs[i, :, spot(core * HALF + place * 256, 256, 256)]
@@ -199,17 +222,75 @@
             part[i, :, at(d, 256)] = turned(own, xs[i, :, at(block, 256)]).astype(BF)
         return scatter_one(source_of(i), [near.at[i, p] for p in range(2)])
 
-    ones = [panel(0)]
+    def gram_rows(p, i1):
+        return spot(p * 64 + i1 * 16, 16, 16)
+
+    group = at(core, 4)
+
+    class Ring:
+        def __init__(self, axis, index, block, cut):
+            self.next, self.prev = turn(axis, index, 1), turn(axis, index, 3)
+            self.index, self.block, self.cut = index, block, cut
+
+        def start(self):
+            ref = self.block(self.index)
+            self.right = send_to(ref, self.next)
+            self.left = send_to(ref, self.prev)
+
+        def second(self):
+            self.right.wait_recv()
+            self.far = [send_to(self.cut(lax.rem(self.index + 3, 4), 0), self.next)]
+            self.left.wait_recv()
+            self.far.append(send_to(self.cut(lax.rem(self.index + 1, 4), 1), self.prev))
+
+        def finish(self):
+            for copy in self.far:
+                copy.wait_recv()
+
+    def rings(phase, block, cut):
+        return [
+            Ring(*axes[p][phase], functools.partial(block, p), functools.partial(cut, p)) for p in range(2)
+        ]
+
+    def b_small(p, j):
+        return gram_b.at[group, gram_rows(p, axes[p][0][1]), at(j, 256)]
+
+    def b_small_cut(p, j, h):
+        return gram_b.at[at(core * 2 + h, 2), gram_rows(p, axes[p][0][1]), at(j, 256)]
+
+    def b_large(p, j):
+        return gram_b.at[group, gram_rows(p, j), :]
+
+    def b_large_cut(p, j, h):
+        return gram_b.at[at(core * 2 + h, 2), gram_rows(p, j), :]
+
+    def g_rows(p, j):
+        return spot(axes[p][0][1] * 64 + j * 16, 16, 16)
+
+    def g_small(p, j):
+        return panels.at[core, :, g_rows(p, j), at(p, 640)]
+
+    def g_small_cut(p, j, h):
+        return panels.at[core, at(h, 2), g_rows(p, j), at(p, 640)]
+
+    def g_large(p, j):
+        return panels.at[core, :, at(j, 64), at(p, 640)]
+
+    def g_large_cut(p, j, h):
+        return panels.at[core, at(h, 2), at(j, 64), at(p, 640)]
+
+    small_b, large_b = rings(1, b_small, b_small_cut), rings(0, b_large, b_large_cut)
+    small, large = rings(1, g_small, g_small_cut), rings(0, g_large, g_large_cut)
+    lines[0][1]()
+    lines[0][2]()
+    part_b[...] = turned(xb[:, spot(core * 512 + place * 128, 128, 128)], xb[...]).astype(BF)
+    one_b = scatter_one(source_b, [near_b.at[p] for p in range(2)])
+    lines[1][1]()
     two_b = []
     for p in range(2):
         kept_b[p] = total(part_b[spot(p * 64 + axes[p][0][1] * 16, 16, 16), :], near_b.at[p], one_b[p])
         two_b.append(exchange(lambda t, p=p: kept_b.at[p, :, at(t, 256)], near2_b.at[p], *axes[p][1]))
-    ones.append(panel(1))
-
-    def gram_rows(p, i1):
-        return spot(p * 64 + i1 * 16, 16, 16)
-
-    group = at(core, 4)
+    lines[2][1]()
     swaps_b = []
     for p in range(2):
         i1, i2 = axes[p][0][1], axes[p][1][1]
@@ -218,73 +299,26 @@
         )
         ref = gram_b.at[core * 4 + place, gram_rows(p, i1), at(i2, 256)]
         swaps_b.append([send_to(ref, {"tp": x}) for x in (across, ahead, behind)])
-    twos = []
-    for i in range(2):
+    for source, target in ((speed_b, branch_m), (speed.at[0], gate_m), (speed.at[1], up_m)):
+        store(source, target)
+    ones = [panel(0), panel(1)]
+
+    def scatter_two(i):
         pair = []
         for p in range(2):
             index = axes[p][0][1]
             kept[i, p] = total(part[i, at(index, 64), at(p, 640)], near.at[i, p], ones[i][p])
-            pair.append(exchange(lambda t, i=i, p=p: kept.at[i, p, at(t, 16), :], near2.at[i, p], *axes[p][1]))
-        twos.append(pair)
-
-    class Ring:
-        def __init__(self, axis, index, block, cut):
-            self.next, self.prev = turn(axis, index, 1), turn(axis, index, 3)
-            self.index, self.block, self.cut = index, block, cut
-
-        def start(self):
-            ref = self.block(self.index)
-            self.right = send_to(ref, self.next)
-            self.left = send_to(ref, self.prev)
-
-        def second(self):
-            self.right.wait_recv()
-            self.far = [send_to(self.cut(lax.rem(self.index + 3, 4), 0), self.next)]
-            self.left.wait_recv()
-            self.far.append(send_to(self.cut(lax.rem(self.index + 1, 4), 1), self.prev))
-
-        def finish(self):
-            for copy in self.far:
-                copy.wait_recv()
-
-    def rings(phase, block, cut):
-        return [
-            Ring(*axes[p][phase], functools.partial(block, p), functools.partial(cut, p)) for p in range(2)
-        ]
-
-    def b_small(p, j):
-        return gram_b.at[group, gram_rows(p, axes[p][0][1]), at(j, 256)]
-
-    def b_small_cut(p, j, h):
-        return gram_b.at[at(core * 2 + h, 2), gram_rows(p, axes[p][0][1]), at(j, 256)]
-
-    def b_large(p, j):
-        return gram_b.at[group, gram_rows(p, j), :]
-
-    def b_large_cut(p, j, h):
-        return gram_b.at[at(core * 2 + h, 2), gram_rows(p, j), :]
-
-    def g_rows(p, j):
-        return spot(axes[p][0][1] * 64 + j * 16, 16, 16)
-
-    def g_small(p, j):
-        return panels.at[core, :, g_rows(p, j), at(p, 640)]
-
-    def g_small_cut(p, j, h):
-        return panels.at[core, at(h, 2), g_rows(p, j), at(p, 640)]
-
-    def g_large(p, j):
-        return panels.at[core, :, at(j, 64), at(p, 640)]
-
-    def g_large_cut(p, j, h):
-        return panels.at[core, at(h, 2), at(j, 64), at(p, 640)]
-
-    small_b, large_b = rings(1, b_small, b_small_cut), rings(0, b_large, b_large_cut)
-    small, large = rings(1, g_small, g_small_cut), rings(0, g_large, g_large_cut)
+            pair.append(exchange(lambda t, p=p: kept.at[i, p, at(t, 16), :], near2.at[i, p], *axes[p][1]))
+        return pair
+
+    twos = [scatter_two(0)]
     for p in range(2):
         for copy in swaps_b[p]:
             copy.wait_recv()
         small_b[p].start()
+    twos.append(scatter_two(1))
+    for ring in small_b:
+        ring.second()
     swaps = []
     for p in range(2):
         i2 = axes[p][1][1]
@@ -298,28 +332,26 @@
             copy.start()
             swaps.append(copy)
     for ring in small_b:
-        ring.second()
+        ring.finish()
+    for ring in large_b:
+        ring.start()
     for copy in swaps:
         copy.wait_recv()
     for ring in small:
         ring.start()
-    for ring in small_b:
-        ring.finish()
-    for ring in large_b:
-        ring.start()
-    for ring in small:
-        ring.second()
     forward_b, forward = [], []
     for p, ring in enumerate(large_b):
         ring.second()
         forward_b += [send_to(b_large(p, lax.rem(ring.index + k, 4)), partner) for k in (0, 3, 1)]
     for ring in small:
+        ring.second()
+    for p, ring in enumerate(large_b):
+        ring.finish()
+        forward_b.append(send_to(b_large(p, lax.rem(ring.index + 2, 4)), partner))
+    for ring in small:
         ring.finish()
     for ring in large:
         ring.start()
-    for p, ring in enumerate(large_b):
-        ring.finish()
-        forward_b.append(send_to(b_large(p, lax.rem(ring.index + 2, 4)), partner))
     for copy in forward_b:
         copy.wait_recv()
 
@@ -381,9 +413,8 @@
     for p in range(2):
         cols = spot(p * 512 + place * 128, 128, 128)
         last_b = COEF_ONE * t_b[0:rows_b, cols].astype(jnp.float32) + dot(line, m_b[:, cols])
-        branch_out[:, at(p, 128)] = SHRINK * branch_w[:, at(p, 128)] - RATE * math.sqrt(D) * last_b.astype(BF).astype(
-            jnp.float32
-        )
+        results_b[:, at(p, 128)] = last_b.astype(BF)
+    store(results_b, branch_out)
     for copy in forward:
         copy.wait_recv()
 
@@ -482,39 +513,66 @@
             src_ref=final.at[2], dst_ref=final.at[4 + i], send_sem=sems.at[COPIES], recv_sem=recvs.at[COPIES + i],
             device_id=partner, device_id_type=MESH,
         ).wait_recv()
-    size = RATE * math.sqrt(FF)
     for i in range(2):
         cols = pl.ds(i * 256, 256)
-        owned = final[i].astype(jnp.float32)
-        fetched = final[4 + i].astype(jnp.float32)
-        even = kind == 0
-        gate_out[:, cols] = SHRINK * gate_w[:, cols] - size * jnp.where(even, owned, fetched)
-        up_out[:, cols] = SHRINK * up_w[:, cols] - size * jnp.where(even, fetched, owned)
+        results[kind, :, cols] = final[i]
+        results[1 - kind, :, cols] = final[4 + i]
+    store(results.at[0], gate_out)
+    store(results.at[1], up_out)
     to_ahead.wait_send()
     to_behind.wait_send()
     for copy in used:
         copy.wait_send()
+    for copy in stores:
+        copy.wait()
+
+
+def finish_kernel(*refs):
+    ins, outs, stage, fresh, in_sem, out_sem = refs[:9], refs[9:15], refs[15:24], refs[24:27], refs[27], refs[28]
+    loads = [pltpu.make_async_copy(ins[i], stage[i], in_sem.at[i]) for i in range(9)]
+    for i in (3, 6, 4, 7, 5, 8, 0, 1, 2):
+        loads[i].start()
+    stores = []
+
+    def store(source, target):
+        copy = pltpu.make_async_copy(source, target, out_sem.at[len(stores)])
+        copy.start()
+        stores.append(copy)
+
+    for i, height in enumerate((FF, FF, D)):
+        loads[3 + i].wait()
+        loads[6 + i].wait()
+        fresh[i][...] = SHRINK * stage[6 + i][...] - RATE * math.sqrt(height) * stage[3 + i][...].astype(jnp.float32)
+        store(fresh[i], outs[2 * i + 1])
+    for i in range(3):
+        loads[i].wait()
+        store(stage[i], outs[2 * i])
+    for copy in stores:
+        copy.wait()
 
 
 def local(*args):
     velocities = (args[1], args[4], args[7])
-    rows, width = velocities[0].shape
-    rows_b, width_b = velocities[2].shape
-    whole = pl.BlockSpec(memory_space=pltpu.VMEM)
+    shapes = [velocity.shape for velocity in velocities]
+    (rows, width), (rows_b, width_b) = shapes[0], shapes[2]
+    anywhere = pl.BlockSpec(memory_space=pl.ANY)
     dma = pltpu.SemaphoreType.DMA
 
     def buf(*shape):
         return pltpu.VMEM(shape, BF)
 
-    outs = []
-    for velocity in velocities:
-        outs += [jax.ShapeDtypeStruct(velocity.shape, jnp.float32)] * 2
-    return pl.pallas_call(
+    def full(*shape):
+        return pltpu.VMEM(shape, jnp.float32)
+
+    outs = [jax.ShapeDtypeStruct(shape, kind) for kind in (jnp.float32, BF) for shape in shapes]
+    middle = pl.pallas_call(
         kernel,
         out_shape=outs,
-        in_specs=[whole] * 9,
-        out_specs=[whole] * 6,
+        in_specs=[anywhere] * 6,
+        out_specs=[anywhere] * 6,
         scratch_shapes=[
+            full(2, 2, rows, width), full(2, rows_b, width_b), full(2, rows, width), full(rows_b, width_b),
+            buf(2, rows, width), buf(rows_b, width_b), dma((9,)), dma((6,)),
             buf(N, N), buf(N, N), buf(N, N), buf(N, HALF),
             buf(2, 2 * rows, N), buf(2 * rows_b, NB), buf(2 * rows, N), buf(2 * rows, N), buf(7, rows, 256),
             buf(2, rows, width), buf(2, rows, width), buf(rows_b, width_b), buf(rows_b, width_b),
@@ -524,8 +582,17 @@
             buf(NB, NB), buf(NB, NB), buf(NB, NB),
             dma((COPIES + 2,)), dma((COPIES + 2,)), dma((4, STEPS)), dma((4, STEPS)),
         ],
-        compiler_params=pltpu.CompilerParams(collective_id=0, has_side_effects=True, vmem_limit_bytes=63 * 1024 * 1024),
-    )(args[0], args[3], args[6], args[1], args[4], args[7], args[2], args[5], args[8])
+        compiler_params=pltpu.CompilerParams(collective_id=0, has_side_effects=True, vmem_limit_bytes=62 * 1024 * 1024),
+    )(args[0], args[3], args[6], args[1], args[4], args[7])
+    results = [jax.ShapeDtypeStruct(shape, jnp.float32) for shape in shapes for _ in range(2)]
+    stage = [full(*shape) for shape in shapes] + [buf(*shape) for shape in shapes] + [full(*shape) for shape in shapes] * 2
+    return pl.pallas_call(
+        finish_kernel,
+        out_shape=results,
+        in_specs=[anywhere] * 9,
+        out_specs=[anywhere] * 6,
+        scratch_shapes=stage + [dma((9,)), dma((6,))],
+    )(*middle, args[2], args[5], args[8])
 
 
 def solution(mesh):

time: 168 us -> 160 us (0.952)
  local copies, waits for them, and re-layouts: 6.38 us -> 0 us
  Pallas kernels: 161 us -> 159 us
    unnamed x16 -> x0, local copies, waits for them, and re-layouts: 6.38 us -> none
    pallas_call x1 -> x2, Pallas kernels: 161 us -> 159 us  [the longest x1 156 us: local(): pl.pallas_call(kernel, out_shape=outs, in_specs=[anywhere] * 6, out_specs...]
where the time goes in v4:
time: 160 us
  Pallas kernels  159 us (99%)
    pallas_call x1, Pallas kernels, local(): pl.pallas_call(kernel, out_shape=outs, in_specs=[anywhere] * 6, out_specs...  156 us

profile of v4, /device:TPU:1, one launch (start us, length us, event | category | flops | bytes accessed | tf_op | source)
XLA Modules:
  0.0 159.7 jit_solution(10963860590701944947)
XLA Ops:
  0.6 156.5 %shard_map.136 = (f32[176,512]{1,0:T(8,128)}, f32[176,512]{1,0:T(8,128)}, f32[64,256]{1,0:T(8,128)}, bf16[176,512]{1,0:T(8,128)(2,1)}, bf16[176,512]{1,0:T(8,128)(2,1)}, /*index=5*/bf16[64,256]{1,0:T(8,128)(2,1)}) custom-call(f32[1,352,512]{2,1,0:T(8,128)} %gate_g.1, f32[1,352,512]{2,1,0:T(8,128)} %up_g.1, f32[1,128,256]{2,1,0:T(8,128)} %branch_g.1, ...), custom_call_target="tpu_custom_call" | custom-call | tf_op jit(solution)/shard_map/pallas_call | solution.py:568
  157.1 2.4 %shard_map.137 = (f32[176,512]{1,0:T(8,128)}, f32[176,512]{1,0:T(8,128)}, f32[176,512]{1,0:T(8,128)}, f32[176,512]{1,0:T(8,128)}, f32[64,256]{1,0:T(8,128)}, /*index=5*/f32[64,256]{1,0:T(8,128)}) custom-call(f32[176,512]{1,0:T(8,128)} %get-tuple-element.12.refs_0_, f32[176,512]{1,0:T(8,128)} %get-tuple-element.13.refs_1_, ...), custom_call_target="tpu_custom_call" | custom-call | tf_op jit(solution)/shard_map/pallas_call | solution.py:589

commit v5 on v4

--- a/solution.py
+++ b/solution.py
@@ -30,8 +30,7 @@
 
 N = 2048
 HALF = 1024
-CHUNK = 512
-STEPS = N // CHUNK
+BLOCK = 512
 NB = 1024
 COPIES = 160
 MESH = pl.DeviceIdType.MESH
@@ -57,7 +56,7 @@
     give, take, give_b, take_b,
     part, near, kept, near2, piece, panels,
     part_b, near_b, kept_b, near2_b, gram_b, m_b, t_b, g_b,
-    sems, recvs, send, recv,
+    stage, sems, recvs, send, recv,
 ):
     core = lax.axis_index("rep")
     place = lax.axis_index("tp")
@@ -440,50 +439,132 @@
 
     x0 = xs.at[kind]
 
-    def swap(buf, k, r, half):
-        ref = buf.at[at(r, CHUNK), at(half, HALF)]
+    def h(q):
+        return at(2 * core + q, BLOCK)
+
+    def o(q):
+        return at(2 * other + q, BLOCK)
+
+    def flip(q):
+        return lax.rem(q + core, 2)
+
+    def flop(q):
+        return lax.rem(q + other, 2)
+
+    def pair(ref, target, k, q):
         return pltpu.make_async_remote_copy(
-            src_ref=ref, dst_ref=ref, send_sem=send.at[k, r], recv_sem=recv.at[k, r], device_id=partner, device_id_type=MESH
+            src_ref=ref, dst_ref=target, send_sem=send.at[k, q], recv_sem=recv.at[k, q], device_id=partner, device_id_type=MESH
         )
 
-    def square(left, k, low, high):
-        def step(r, _):
-            if k is not None:
-                swap(left, k, r, core).wait_send()
-                swap(left, k, r, other).wait_recv()
-            s = dot(left[at(r, CHUNK), :], left[:, mine])
-            m[at(r, CHUNK), :] = (low * left[at(r, CHUNK), mine].astype(jnp.float32) + high * s).astype(BF)
+    def cross_out(buf, k, q):
+        ref = buf.at[o(q), h(flip(q))]
+        return pair(ref, ref, k, q)
+
+    def cross_in(buf, k, q):
+        ref = buf.at[h(q), o(flop(q))]
+        return pair(ref, ref, k, q)
+
+    def square_out(buf, k, q, side):
+        first = at(2 * side, BLOCK)
+        second = at(2 * side + 1, BLOCK)
+        ref = (buf.at[first, at(side, HALF)], buf.at[second, first], buf.at[second, second])[q]
+        return pair(ref, ref, k, 2 + q)
+
+    def stage_out(k, q):
+        return pair(m.at[o(q), at(flip(q), BLOCK)], stage.at[q], 4 + k, q)
+
+    def product(left, k, right, emit, after_head, after_cross, after_all):
+        if k is not None:
+            def receive(q, _):
+                cross_out(left, k, q).wait_send()
+                cross_in(left, k, q).wait_recv()
+                left[o(flop(q)), h(q)] = left[h(q), o(flop(q))].T
+                return 0
+
+            lax.fori_loop(0, 2, receive, 0)
+
+        def head(q, _):
+            emit(h(q), 0, dot(left[h(q), :], right(0)))
             return 0
 
-        lax.fori_loop(0, STEPS, step, 0)
+        lax.fori_loop(0, 2, head, 0)
+        after_head()
+        if k is not None:
+            for q in range(3):
+                square_out(left, k, q, core).wait_send()
+                square_out(left, k, q, other).wait_recv()
+
+        def cross(q, _):
+            j = flip(q)
+            emit(o(q), j, dot(left[o(q), :], right(j)))
+            after_cross(q)
+            return 0
+
+        lax.fori_loop(0, 2, cross, 0)
+        emit(h(1), 1, dot(left[h(1), :], right(1)))
+        after_all()
+
+    def square(left, k, k_out, low, high):
+        def emit(where, j, value):
+            value = low * left[where, h(j)].astype(jnp.float32) + high * value
+            m[where, at(j, BLOCK)] = value.astype(BF)
+
+        def after_head():
+            m[h(0), at(1, BLOCK)] = m[h(1), at(0, BLOCK)].T
+
+        def after_cross(q):
+            stage_out(k_out, q).start()
+
+        def right(j):
+            return left[:, h(j)]
+
+        product(left, k, right, emit, after_head, after_cross, lambda: None)
+
+        def receive(q, _):
+            copy = stage_out(k_out, q)
+            copy.wait_send()
+            copy.wait_recv()
+            m[o(flop(q)), at(q, BLOCK)] = stage[q].T
+            return 0
+
+        lax.fori_loop(0, 2, receive, 0)
 
     def times(left, k, out, k_out, factor):
-        def step(r, _):
-            if k is not None:
-                swap(left, k, r, core).wait_send()
-                swap(left, k, r, other).wait_recv()
-            p = dot(left[at(r, CHUNK), :], m[...])
-            p = COEF_ONE * left[at(r, CHUNK), mine].astype(jnp.float32) + p
+        def emit(where, j, value):
+            value = COEF_ONE * left[where, h(j)].astype(jnp.float32) + value
             if factor is not None:
-                p = factor * p
-            out[at(r, CHUNK), mine] = p.astype(BF)
-            swap(out, k_out, r, core).start()
-            return 0
-
-        lax.fori_loop(0, STEPS, step, 0)
-
-    square(a, None, COEF_THREE * alpha, COEF_FIVE * alpha * alpha)
+                value = factor * value
+            out[where, h(j)] = value.astype(BF)
+
+        def after_head():
+            out[h(0), h(1)] = out[h(1), h(0)].T
+            square_out(out, k_out, 0, core).start()
+            square_out(out, k_out, 1, core).start()
+
+        def after_cross(q):
+            cross_out(out, k_out, q).start()
+            out[h(flip(q)), o(q)] = out[o(q), h(flip(q))].T
+
+        def after_all():
+            square_out(out, k_out, 2, core).start()
+
+        def right(j):
+            return m[:, at(j, BLOCK)]
+
+        product(left, k, right, emit, after_head, after_cross, after_all)
+
+    square(a, None, 0, COEF_THREE * alpha, COEF_FIVE * alpha * alpha)
     times(a, None, b, 0, alpha)
     x1[:, mine] = (scale * (COEF_ONE * x0[:, mine].astype(jnp.float32) + dot(x0[...], m[...]))).astype(BF)
     turn_one = send_to(x1.at[:, mine], partner)
     times(b, 0, c, 1, None)
-    square(c, 1, COEF_THREE, COEF_FIVE)
+    square(c, 1, 1, COEF_THREE, COEF_FIVE)
     times(c, None, b, 2, None)
     turn_one.wait_recv()
     x2[:, mine] = (COEF_ONE * x1[:, mine].astype(jnp.float32) + dot(x1[...], m[...])).astype(BF)
     turn_two = send_to(x2.at[:, mine], partner)
     times(b, 2, a, 3, None)
-    square(a, 3, COEF_THREE, COEF_FIVE)
+    square(a, 3, 2, COEF_THREE, COEF_FIVE)
     turn_two.wait_recv()
 
     def last(where, block):
@@ -580,7 +661,8 @@
             buf(2, 4, 256, 1280),
             buf(128, NB), buf(2, 3, 16, NB), buf(2, 16, NB), buf(2, 3, 16, 256), buf(8, 128, NB),
             buf(NB, NB), buf(NB, NB), buf(NB, NB),
-            dma((COPIES + 2,)), dma((COPIES + 2,)), dma((4, STEPS)), dma((4, STEPS)),
+            buf(2, BLOCK, BLOCK),
+            dma((COPIES + 2,)), dma((COPIES + 2,)), dma((7, 5)), dma((7, 5)),
         ],
         compiler_params=pltpu.CompilerParams(collective_id=0, has_side_effects=True, vmem_limit_bytes=62 * 1024 * 1024),
     )(args[0], args[3], args[6], args[1], args[4], args[7])

time: 160 us -> 146 us (0.912)
  Pallas kernels: 159 us -> 145 us
    pallas_call x1, Pallas kernels: 156 us -> 143 us  [local(): pl.pallas_call(kernel, out_shape=outs, in_specs=[anywhere] * 6, out_specs...]
where the time goes in v5:
time: 146 us
  Pallas kernels  145 us (99%)
    pallas_call x1, Pallas kernels, local(): pl.pallas_call(kernel, out_shape=outs, in_specs=[anywhere] * 6, out_specs...  143 us

profile of v5, /device:TPU:1, one launch (start us, length us, event | category | flops | bytes accessed | tf_op | source)
XLA Modules:
  0.0 145.8 jit_solution(3600984866808469748)
XLA Ops:
  0.6 142.6 %shard_map.136 = (f32[176,512]{1,0:T(8,128)}, f32[176,512]{1,0:T(8,128)}, f32[64,256]{1,0:T(8,128)}, bf16[176,512]{1,0:T(8,128)(2,1)}, bf16[176,512]{1,0:T(8,128)(2,1)}, /*index=5*/bf16[64,256]{1,0:T(8,128)(2,1)}) custom-call(f32[1,352,512]{2,1,0:T(8,128)} %gate_g.1, f32[1,352,512]{2,1,0:T(8,128)} %up_g.1, f32[1,128,256]{2,1,0:T(8,128)} %branch_g.1, ...), custom_call_target="tpu_custom_call" | custom-call | tf_op jit(solution)/shard_map/pallas_call | solution.py:649
  143.2 2.4 %shard_map.137 = (f32[176,512]{1,0:T(8,128)}, f32[176,512]{1,0:T(8,128)}, f32[176,512]{1,0:T(8,128)}, f32[176,512]{1,0:T(8,128)}, f32[64,256]{1,0:T(8,128)}, /*index=5*/f32[64,256]{1,0:T(8,128)}) custom-call(f32[176,512]{1,0:T(8,128)} %get-tuple-element.12.refs_0_, f32[176,512]{1,0:T(8,128)} %get-tuple-element.13.refs_1_, ...), custom_call_target="tpu_custom_call" | custom-call | tf_op jit(solution)/shard_map/pallas_call | solution.py:671

commit v6 on v5

--- a/solution.py
+++ b/solution.py
@@ -52,9 +52,9 @@
     gate_g, up_g, branch_g, gate_v, up_v, branch_v,
     gate_m, up_m, branch_m, gate_out, up_out, branch_out,
     grads, grads_b, speed, speed_b, results, results_b, in_sem, out_sem,
-    a, b, c, m, xs, xb, x1, x2, final,
+    a, b, c, m, x0, xb, x1, x2, final, starts, relay,
     give, take, give_b, take_b,
-    part, near, kept, near2, piece, panels,
+    part, near, kept, near2, panels,
     part_b, near_b, kept_b, near2_b, gram_b, m_b, t_b, g_b,
     stage, sems, recvs, send, recv,
 ):
@@ -158,8 +158,44 @@
 
         return start, second, finish
 
-    gate_x, up_x = xs.at[0], xs.at[1]
-    lines = [columns(xb, None, rows_b, 128), columns(gate_x, None, rows, 256), columns(up_x, None, rows, 256)]
+    lines = [columns(xb, None, rows_b, 128)]
+    line = {}
+
+    def block_of(x, p):
+        return x0.at[own_rows, spot(p * HALF + x * 256, 256, 256)]
+
+    def line_start():
+        line["relay"] = [
+            remote(starts.at[kind, p], relay.at[p], {"tp": to}) for p, to in ((0, ahead), (1, behind))
+        ]
+        line["out"] = [
+            [remote(starts.at[1 - kind, p], block_of(place, p), {"tp": to}) for p in range(2)] for to in (ahead, behind)
+        ]
+        for copy in line["relay"] + line["out"][0] + line["out"][1]:
+            copy.start()
+        line["own"] = [send_to(block_of(place, p), partner) for p in range(2)]
+
+    def line_second():
+        line["far"] = []
+        for p, (source, to) in enumerate(((behind, ahead), (ahead, behind))):
+            line["relay"][p].wait_recv()
+            copy = remote(relay.at[p], block_of(source, p), {"tp": to})
+            copy.start()
+            line["far"].append(copy)
+
+    def line_third():
+        for side, source in ((0, behind), (1, ahead)):
+            for p in range(2):
+                line["out"][side][p].wait_recv()
+                line["own"].append(send_to(block_of(source, p), partner))
+
+    def line_finish():
+        for p in range(2):
+            line["far"][p].wait_recv()
+            line["own"].append(send_to(block_of(across, p), partner))
+        for copy in line["own"]:
+            copy.wait_recv()
+
     first_copies[0].wait_recv()
     loads[3].wait()
     loads[4].wait()
@@ -175,8 +211,10 @@
         moment = MOMENT * speed[i] + (grads[i, 0] + take[i].astype(jnp.float32))
         speed[i] = moment
         for p in range(2):
-            xs[i, own_rows, spot(p * HALF + place * 256, 256, 256)] = moment[:, p * 256 : p * 256 + 256].astype(BF)
-        lines[1 + i][0]()
+            starts[i, p] = moment[:, p * 256 : p * 256 + 256].astype(BF)
+    for p in range(2):
+        x0[own_rows, spot(p * HALF + place * 256, 256, 256)] = starts[kind, p]
+    line_start()
     stores = []
 
     def store(source, target):
@@ -213,12 +251,13 @@
     def source_b(p, t):
         return part_b.at[spot(p * 64 + t * 16, 16, 16), :]
 
+    upper = lax.div(place, 2)
+
     def panel(i):
-        lines[1 + i][2]()
-        own = xs[i, :, spot(core * HALF + place * 256, 256, 256)]
+        first = core * 4 + 2 * upper + i
+        own = x0[:, at(first, 256)]
         for d in range(5):
-            block = lax.rem(core * 4 + place + d, 8)
-            part[i, :, at(d, 256)] = turned(own, xs[i, :, at(block, 256)]).astype(BF)
+            part[i, :, at(d, 256)] = turned(own, x0[:, at(lax.rem(first + d, 8), 256)]).astype(BF)
         return scatter_one(source_of(i), [near.at[i, p] for p in range(2)])
 
     def gram_rows(p, i1):
@@ -284,12 +323,12 @@
     lines[0][2]()
     part_b[...] = turned(xb[:, spot(core * 512 + place * 128, 128, 128)], xb[...]).astype(BF)
     one_b = scatter_one(source_b, [near_b.at[p] for p in range(2)])
-    lines[1][1]()
+    line_second()
     two_b = []
     for p in range(2):
         kept_b[p] = total(part_b[spot(p * 64 + axes[p][0][1] * 16, 16, 16), :], near_b.at[p], one_b[p])
         two_b.append(exchange(lambda t, p=p: kept_b.at[p, :, at(t, 256)], near2_b.at[p], *axes[p][1]))
-    lines[2][1]()
+    line_third()
     swaps_b = []
     for p in range(2):
         i1, i2 = axes[p][0][1], axes[p][1][1]
@@ -300,6 +339,7 @@
         swaps_b.append([send_to(ref, {"tp": x}) for x in (across, ahead, behind)])
     for source, target in ((speed_b, branch_m), (speed.at[0], gate_m), (speed.at[1], up_m)):
         store(source, target)
+    line_finish()
     ones = [panel(0), panel(1)]
 
     def scatter_two(i):
@@ -322,14 +362,10 @@
     for p in range(2):
         i2 = axes[p][1][1]
         for i in range(2):
-            piece[i, p] = total(kept[i, p, at(i2, 16), :], near2.at[i, p], twos[i][p])
-        target = panels.at[core, place, g_rows(p, i2), at(p, 640)]
-        panels[core, place, g_rows(p, i2), at(p, 640)] = piece[kind, p]
-        swaps.append(send_to(target, {"tp": across}))
-        for x in (ahead, behind):
-            copy = remote(piece.at[1 - kind, p], target, {"tp": x})
-            copy.start()
-            swaps.append(copy)
+            panels[core, 2 * upper + i, g_rows(p, i2), at(p, 640)] = total(
+                kept[i, p, at(i2, 16), :], near2.at[i, p], twos[i][p]
+            )
+        swaps.append(send_to(panels.at[core, at(upper, 2), g_rows(p, i2), at(p, 640)], {"tp": across}))
     for ring in small_b:
         ring.finish()
     for ring in large_b:
@@ -371,22 +407,18 @@
     sums = lax.fori_loop(0, 8, squares_b, (jnp.zeros((8, NB), jnp.float32), jnp.zeros((128, 128), jnp.float32)))
     alpha_b, scale_b = coefficients(jnp.sum(sums[0]), jnp.sum(sums[1]))
 
+    top, low_half = pl.ds(0, 512), pl.ds(512, 512)
+
+    def mirrored_b(left, right, out, emit):
+        out[top, top] = emit(left[top, top], dot(left[top, :], right[:, top])).astype(BF)
+        out[low_half, :] = emit(left[low_half, :], dot(left[low_half, :], right[...])).astype(BF)
+        out[top, low_half] = out[low_half, top].T
+
     def square_b(left, low, high):
-        def step(r, _):
-            where = at(r, 512)
-            m_b[where, :] = (low * left[where, :].astype(jnp.float32) + high * dot(left[where, :], left[...])).astype(BF)
-            return 0
-
-        lax.fori_loop(0, 2, step, 0)
+        mirrored_b(left, left, m_b, lambda own, value: low * own.astype(jnp.float32) + high * value)
 
     def times_b(left, out, factor):
-        def step(r, _):
-            where = at(r, 512)
-            value = factor * (COEF_ONE * left[where, :].astype(jnp.float32) + dot(left[where, :], m_b[...]))
-            out[where, :] = value.astype(BF)
-            return 0
-
-        lax.fori_loop(0, 2, step, 0)
+        mirrored_b(left, m_b, out, lambda own, value: factor * (COEF_ONE * own.astype(jnp.float32) + value))
 
     def rows_of(left, factor):
         return (factor * (COEF_ONE * left.astype(jnp.float32) + dot(left, m_b[...]))).astype(BF)
@@ -395,23 +427,23 @@
         g_b[at(i, 128), :] = gram_b[i]
     square_b(g_b, COEF_THREE * alpha_b, COEF_FIVE * alpha_b * alpha_b)
     times_b(g_b, t_b, alpha_b)
-    line = rows_of(xb[at(core, rows_b), :], scale_b)
+    line_b = rows_of(xb[at(core, rows_b), :], scale_b)
     times_b(t_b, g_b, 1.0)
     square_b(g_b, COEF_THREE, COEF_FIVE)
     for p, ring in enumerate(large):
         ring.second()
         forward += [send_to(g_large(p, lax.rem(ring.index + k, 4)), partner) for k in (0, 3, 1)]
     times_b(g_b, t_b, 1.0)
-    line = rows_of(line, 1.0)
+    line_b = rows_of(line_b, 1.0)
     times_b(t_b, g_b, 1.0)
     for p, ring in enumerate(large):
         ring.finish()
         forward.append(send_to(g_large(p, lax.rem(ring.index + 2, 4)), partner))
     square_b(g_b, COEF_THREE, COEF_FIVE)
-    t_b[0:rows_b, :] = line
+    t_b[0:rows_b, :] = line_b
     for p in range(2):
         cols = spot(p * 512 + place * 128, 128, 128)
-        last_b = COEF_ONE * t_b[0:rows_b, cols].astype(jnp.float32) + dot(line, m_b[:, cols])
+        last_b = COEF_ONE * t_b[0:rows_b, cols].astype(jnp.float32) + dot(line_b, m_b[:, cols])
         results_b[:, at(p, 128)] = last_b.astype(BF)
     store(results_b, branch_out)
     for copy in forward:
@@ -437,7 +469,6 @@
     sums = lax.fori_loop(0, 8, assemble, (jnp.zeros((8, 256), jnp.float32), jnp.zeros((128, 128), jnp.float32)))
     alpha, scale = coefficients(jnp.sum(sums[0]), jnp.sum(sums[1]))
 
-    x0 = xs.at[kind]
 
     def h(q):
         return at(2 * core + q, BLOCK)
@@ -473,15 +504,23 @@
     def stage_out(k, q):
         return pair(m.at[o(q), at(flip(q), BLOCK)], stage.at[q], 4 + k, q)
 
+    def receive_cross(left, k):
+        def step(q, _):
+            cross_out(left, k, q).wait_send()
+            cross_in(left, k, q).wait_recv()
+            left[o(flop(q)), h(q)] = left[h(q), o(flop(q))].T
+            return 0
+
+        lax.fori_loop(0, 2, step, 0)
+
+    def receive_square(left, k):
+        for q in range(3):
+            square_out(left, k, q, core).wait_send()
+            square_out(left, k, q, other).wait_recv()
+
     def product(left, k, right, emit, after_head, after_cross, after_all):
         if k is not None:
-            def receive(q, _):
-                cross_out(left, k, q).wait_send()
-                cross_in(left, k, q).wait_recv()
-                left[o(flop(q)), h(q)] = left[h(q), o(flop(q))].T
-                return 0
-
-            lax.fori_loop(0, 2, receive, 0)
+            receive_cross(left, k)
 
         def head(q, _):
             emit(h(q), 0, dot(left[h(q), :], right(0)))
@@ -490,9 +529,7 @@
         lax.fori_loop(0, 2, head, 0)
         after_head()
         if k is not None:
-            for q in range(3):
-                square_out(left, k, q, core).wait_send()
-                square_out(left, k, q, other).wait_recv()
+            receive_square(left, k)
 
         def cross(q, _):
             j = flip(q)
@@ -564,26 +601,42 @@
     x2[:, mine] = (COEF_ONE * x1[:, mine].astype(jnp.float32) + dot(x1[...], m[...])).astype(BF)
     turn_two = send_to(x2.at[:, mine], partner)
     times(b, 2, a, 3, None)
-    square(a, 3, 2, COEF_THREE, COEF_FIVE)
-    turn_two.wait_recv()
+
+    def some(block, low, high):
+        close = spot(core * HALF + block * 256, 256, 256)
+
+        def step(r, _):
+            where = at(lax.rem(2 * core + r, 4), BLOCK)
+            value = COEF_THREE * a[where, close].astype(jnp.float32) + COEF_FIVE * dot(a[where, :], a[:, close])
+            m[where, at(block, 256)] = value.astype(BF)
+            return 0
+
+        lax.fori_loop(low, high, step, 0)
 
     def last(where, block):
         cols = at(block, 256)
         close = spot(core * HALF + block * 256, 256, 256)
         return (COEF_ONE * x2[where, close].astype(jnp.float32) + dot(x2[where, :], m[:, cols])).astype(BF)
 
+    receive_cross(a, 3)
+    some(ahead, 0, 2)
+    receive_square(a, 3)
+    some(ahead, 2, 4)
+    turn_two.wait_recv()
     final[2] = last(pl.ds(0, rows), ahead)
     to_ahead = pltpu.make_async_remote_copy(
         src_ref=final.at[2], dst_ref=final.at[4 + core], send_sem=sems.at[COPIES], recv_sem=recvs.at[COPIES + core],
         device_id={"tp": ahead, "rep": 0}, device_id_type=MESH,
     )
     to_ahead.start()
+    some(behind, 0, 4)
     final[3] = last(pl.ds(rows, rows), behind)
     to_behind = pltpu.make_async_remote_copy(
         src_ref=final.at[3], dst_ref=final.at[4 + core], send_sem=sems.at[COPIES + 1], recv_sem=recvs.at[COPIES + core],
         device_id={"tp": behind, "rep": 1}, device_id_type=MESH,
     )
     to_behind.start()
+    some(place, 0, 4)
     final[6] = last(other_rows, place)
     to_partner = remote(final.at[6], final.at[core], partner)
     to_partner.start()
@@ -655,9 +708,10 @@
             full(2, 2, rows, width), full(2, rows_b, width_b), full(2, rows, width), full(rows_b, width_b),
             buf(2, rows, width), buf(rows_b, width_b), dma((9,)), dma((6,)),
             buf(N, N), buf(N, N), buf(N, N), buf(N, HALF),
-            buf(2, 2 * rows, N), buf(2 * rows_b, NB), buf(2 * rows, N), buf(2 * rows, N), buf(7, rows, 256),
+            buf(2 * rows, N), buf(2 * rows_b, NB), buf(2 * rows, N), buf(2 * rows, N), buf(7, rows, 256),
+            buf(2, 2, rows, 256), buf(2, rows, 256),
             buf(2, rows, width), buf(2, rows, width), buf(rows_b, width_b), buf(rows_b, width_b),
-            buf(2, 256, 1280), buf(2, 2, 3, 64, 640), buf(2, 2, 64, 640), buf(2, 2, 3, 16, 640), buf(2, 2, 16, 640),
+            buf(2, 256, 1280), buf(2, 2, 3, 64, 640), buf(2, 2, 64, 640), buf(2, 2, 3, 16, 640),
             buf(2, 4, 256, 1280),
             buf(128, NB), buf(2, 3, 16, NB), buf(2, 16, NB), buf(2, 3, 16, 256), buf(8, 128, NB),
             buf(NB, NB), buf(NB, NB), buf(NB, NB),

time: 146 us -> 137 us (0.938)
  Pallas kernels: 145 us -> 136 us
    pallas_call x1, Pallas kernels: 143 us -> 134 us  [local(): pl.pallas_call(kernel, out_shape=outs, in_specs=[anywhere] * 6, out_specs...]
where the time goes in v6:
time: 137 us
  Pallas kernels  136 us (99%)
    pallas_call x1, Pallas kernels, local(): pl.pallas_call(kernel, out_shape=outs, in_specs=[anywhere] * 6, out_specs...  134 us

profile of v6, /device:TPU:1, one launch (start us, length us, event | category | flops | bytes accessed | tf_op | source)
XLA Modules:
  0.0 137.2 jit_solution(13282730402609089572)
XLA Ops:
  0.6 133.9 %shard_map.136 = (f32[176,512]{1,0:T(8,128)}, f32[176,512]{1,0:T(8,128)}, f32[64,256]{1,0:T(8,128)}, bf16[176,512]{1,0:T(8,128)(2,1)}, bf16[176,512]{1,0:T(8,128)(2,1)}, /*index=5*/bf16[64,256]{1,0:T(8,128)(2,1)}) custom-call(f32[1,352,512]{2,1,0:T(8,128)} %gate_g.1, f32[1,352,512]{2,1,0:T(8,128)} %up_g.1, f32[1,128,256]{2,1,0:T(8,128)} %branch_g.1, ...), custom_call_target="tpu_custom_call" | custom-call | tf_op jit(solution)/shard_map/pallas_call | solution.py:702
  134.6 2.4 %shard_map.137 = (f32[176,512]{1,0:T(8,128)}, f32[176,512]{1,0:T(8,128)}, f32[176,512]{1,0:T(8,128)}, f32[176,512]{1,0:T(8,128)}, f32[64,256]{1,0:T(8,128)}, /*index=5*/f32[64,256]{1,0:T(8,128)}) custom-call(f32[176,512]{1,0:T(8,128)} %get-tuple-element.12.refs_0_, f32[176,512]{1,0:T(8,128)} %get-tuple-element.13.refs_1_, ...), custom_call_target="tpu_custom_call" | custom-call | tf_op jit(solution)/shard_map/pallas_call | solution.py:725

commit v7 on v6

--- a/solution.py
+++ b/solution.py
@@ -320,15 +320,19 @@
     small_b, large_b = rings(1, b_small, b_small_cut), rings(0, b_large, b_large_cut)
     small, large = rings(1, g_small, g_small_cut), rings(0, g_large, g_large_cut)
     lines[0][1]()
+    line_second()
     lines[0][2]()
     part_b[...] = turned(xb[:, spot(core * 512 + place * 128, 128, 128)], xb[...]).astype(BF)
     one_b = scatter_one(source_b, [near_b.at[p] for p in range(2)])
-    line_second()
+    line_third()
+    for source, target in ((speed_b, branch_m), (speed.at[0], gate_m), (speed.at[1], up_m)):
+        store(source, target)
+    line_finish()
+    ones = [panel(0), panel(1)]
     two_b = []
     for p in range(2):
         kept_b[p] = total(part_b[spot(p * 64 + axes[p][0][1] * 16, 16, 16), :], near_b.at[p], one_b[p])
         two_b.append(exchange(lambda t, p=p: kept_b.at[p, :, at(t, 256)], near2_b.at[p], *axes[p][1]))
-    line_third()
     swaps_b = []
     for p in range(2):
         i1, i2 = axes[p][0][1], axes[p][1][1]
@@ -337,10 +341,6 @@
         )
         ref = gram_b.at[core * 4 + place, gram_rows(p, i1), at(i2, 256)]
         swaps_b.append([send_to(ref, {"tp": x}) for x in (across, ahead, behind)])
-    for source, target in ((speed_b, branch_m), (speed.at[0], gate_m), (speed.at[1], up_m)):
-        store(source, target)
-    line_finish()
-    ones = [panel(0), panel(1)]
 
     def scatter_two(i):
         pair = []

time: 137 us -> 138 us (level)
  no operation moved by 1% of the time
where the time goes in v7:
time: 138 us
  Pallas kernels  137 us (99%)
    pallas_call x1, Pallas kernels, local(): pl.pallas_call(kernel, out_shape=outs, in_specs=[anywhere] * 6, out_specs...  135 us

profile of v7, /device:TPU:1, one launch (start us, length us, event | category | flops | bytes accessed | tf_op | source)
XLA Modules:
  0.0 138.0 jit_solution(2270725769387142758)
XLA Ops:
  0.6 134.7 %shard_map.136 = (f32[176,512]{1,0:T(8,128)}, f32[176,512]{1,0:T(8,128)}, f32[64,256]{1,0:T(8,128)}, bf16[176,512]{1,0:T(8,128)(2,1)}, bf16[176,512]{1,0:T(8,128)(2,1)}, /*index=5*/bf16[64,256]{1,0:T(8,128)(2,1)}) custom-call(f32[1,352,512]{2,1,0:T(8,128)} %gate_g.1, f32[1,352,512]{2,1,0:T(8,128)} %up_g.1, f32[1,128,256]{2,1,0:T(8,128)} %branch_g.1, ...), custom_call_target="tpu_custom_call" | custom-call | tf_op jit(solution)/shard_map/pallas_call | solution.py:702
  135.4 2.4 %shard_map.137 = (f32[176,512]{1,0:T(8,128)}, f32[176,512]{1,0:T(8,128)}, f32[176,512]{1,0:T(8,128)}, f32[176,512]{1,0:T(8,128)}, f32[64,256]{1,0:T(8,128)}, /*index=5*/f32[64,256]{1,0:T(8,128)}) custom-call(f32[176,512]{1,0:T(8,128)} %get-tuple-element.12.refs_0_, f32[176,512]{1,0:T(8,128)} %get-tuple-element.13.refs_1_, ...), custom_call_target="tpu_custom_call" | custom-call | tf_op jit(solution)/shard_map/pallas_call | solution.py:725

commit v8 on v7

--- a/solution.py
+++ b/solution.py
@@ -327,12 +327,12 @@
     line_third()
     for source, target in ((speed_b, branch_m), (speed.at[0], gate_m), (speed.at[1], up_m)):
         store(source, target)
-    line_finish()
-    ones = [panel(0), panel(1)]
     two_b = []
     for p in range(2):
         kept_b[p] = total(part_b[spot(p * 64 + axes[p][0][1] * 16, 16, 16), :], near_b.at[p], one_b[p])
         two_b.append(exchange(lambda t, p=p: kept_b.at[p, :, at(t, 256)], near2_b.at[p], *axes[p][1]))
+    line_finish()
+    ones = [panel(0), panel(1)]
     swaps_b = []
     for p in range(2):
         i1, i2 = axes[p][0][1], axes[p][1][1]
@@ -350,12 +350,11 @@
             pair.append(exchange(lambda t, p=p: kept.at[i, p, at(t, 16), :], near2.at[i, p], *axes[p][1]))
         return pair
 
-    twos = [scatter_two(0)]
     for p in range(2):
         for copy in swaps_b[p]:
             copy.wait_recv()
         small_b[p].start()
-    twos.append(scatter_two(1))
+    twos = [scatter_two(0), scatter_two(1)]
     for ring in small_b:
         ring.second()
     swaps = []
@@ -370,9 +369,8 @@
         ring.finish()
     for ring in large_b:
         ring.start()
-    for copy in swaps:
+    for copy, ring in zip(swaps, small):
         copy.wait_recv()
-    for ring in small:
         ring.start()
     forward_b, forward = [], []
     for p, ring in enumerate(large_b):
@@ -380,13 +378,13 @@
         forward_b += [send_to(b_large(p, lax.rem(ring.index + k, 4)), partner) for k in (0, 3, 1)]
     for ring in small:
         ring.second()
-    for p, ring in enumerate(large_b):
-        ring.finish()
-        forward_b.append(send_to(b_large(p, lax.rem(ring.index + 2, 4)), partner))
     for ring in small:
         ring.finish()
     for ring in large:
         ring.start()
+    for p, ring in enumerate(large_b):
+        ring.finish()
+        forward_b.append(send_to(b_large(p, lax.rem(ring.index + 2, 4)), partner))
     for copy in forward_b:
         copy.wait_recv()
 

time: 138 us -> 135 us (0.978)
  Pallas kernels: 137 us -> 134 us
    pallas_call x1, Pallas kernels: 135 us -> 132 us  [local(): pl.pallas_call(kernel, out_shape=outs, in_specs=[anywhere] * 6, out_specs...]
where the time goes in v8:
time: 135 us
  Pallas kernels  134 us (99%)
    pallas_call x1, Pallas kernels, local(): pl.pallas_call(kernel, out_shape=outs, in_specs=[anywhere] * 6, out_specs...  132 us

profile of v8, /device:TPU:1, one launch (start us, length us, event | category | flops | bytes accessed | tf_op | source)
XLA Modules:
  0.0 134.9 jit_solution(15470511177557672912)
XLA Ops:
  0.6 131.6 %shard_map.136 = (f32[176,512]{1,0:T(8,128)}, f32[176,512]{1,0:T(8,128)}, f32[64,256]{1,0:T(8,128)}, bf16[176,512]{1,0:T(8,128)(2,1)}, bf16[176,512]{1,0:T(8,128)(2,1)}, /*index=5*/bf16[64,256]{1,0:T(8,128)(2,1)}) custom-call(f32[1,352,512]{2,1,0:T(8,128)} %gate_g.1, f32[1,352,512]{2,1,0:T(8,128)} %up_g.1, f32[1,128,256]{2,1,0:T(8,128)} %branch_g.1, ...), custom_call_target="tpu_custom_call" | custom-call | tf_op jit(solution)/shard_map/pallas_call | solution.py:700
  132.2 2.4 %shard_map.137 = (f32[176,512]{1,0:T(8,128)}, f32[176,512]{1,0:T(8,128)}, f32[176,512]{1,0:T(8,128)}, f32[176,512]{1,0:T(8,128)}, f32[64,256]{1,0:T(8,128)}, /*index=5*/f32[64,256]{1,0:T(8,128)}) custom-call(f32[176,512]{1,0:T(8,128)} %get-tuple-element.12.refs_0_, f32[176,512]{1,0:T(8,128)} %get-tuple-element.13.refs_1_, ...), custom_call_target="tpu_custom_call" | custom-call | tf_op jit(solution)/shard_map/pallas_call | solution.py:723

commit v9 on v8

--- a/solution.py
+++ b/solution.py
@@ -52,11 +52,11 @@
     gate_g, up_g, branch_g, gate_v, up_v, branch_v,
     gate_m, up_m, branch_m, gate_out, up_out, branch_out,
     grads, grads_b, speed, speed_b, results, results_b, in_sem, out_sem,
-    a, b, c, m, x0, xb, x1, x2, final, starts, relay,
+    pairs, b, m, xall, xb, final, starts, relay,
     give, take, give_b, take_b,
     part, near, kept, near2, panels,
     part_b, near_b, kept_b, near2_b, gram_b, m_b, t_b, g_b,
-    stage, sems, recvs, send, recv,
+    stage, sems, recvs, send, recv, xsend, xrecv,
 ):
     core = lax.axis_index("rep")
     place = lax.axis_index("tp")
@@ -88,6 +88,8 @@
     mine = at(core, HALF)
     partner = {"rep": other}
     used = []
+    x0 = xall.at[0]
+    a = pairs.at[0]
 
     def turn(axis, index, step):
         return {axis: lax.rem(index + step, 4)}
@@ -516,30 +518,19 @@
             square_out(left, k, q, core).wait_send()
             square_out(left, k, q, other).wait_recv()
 
-    def product(left, k, right, emit, after_head, after_cross, after_all):
-        if k is not None:
-            receive_cross(left, k)
-
-        def head(q, _):
-            emit(h(q), 0, dot(left[h(q), :], right(0)))
-            return 0
-
-        lax.fori_loop(0, 2, head, 0)
+    def product(left, receive, right, emit, after_head, after_cross, after_all):
+        receive(receive_cross)
+        emit(at(core, HALF), 0, dot(left[at(core, HALF), :], right(0)))
         after_head()
-        if k is not None:
-            receive_square(left, k)
-
-        def cross(q, _):
+        receive(receive_square)
+        for q in range(2):
             j = flip(q)
             emit(o(q), j, dot(left[o(q), :], right(j)))
             after_cross(q)
-            return 0
-
-        lax.fori_loop(0, 2, cross, 0)
         emit(h(1), 1, dot(left[h(1), :], right(1)))
         after_all()
 
-    def square(left, k, k_out, low, high):
+    def square(left, receive, k_out, low, high):
         def emit(where, j, value):
             value = low * left[where, h(j)].astype(jnp.float32) + high * value
             m[where, at(j, BLOCK)] = value.astype(BF)
@@ -553,22 +544,16 @@
         def right(j):
             return left[:, h(j)]
 
-        product(left, k, right, emit, after_head, after_cross, lambda: None)
-
-        def receive(q, _):
+        product(left, receive, right, emit, after_head, after_cross, lambda: None)
+        for q in range(2):
             copy = stage_out(k_out, q)
             copy.wait_send()
             copy.wait_recv()
             m[o(flop(q)), at(q, BLOCK)] = stage[q].T
-            return 0
-
-        lax.fori_loop(0, 2, receive, 0)
-
-    def times(left, k, out, k_out, factor):
+
+    def times(left, receive, out, k_out, factor):
         def emit(where, j, value):
-            value = COEF_ONE * left[where, h(j)].astype(jnp.float32) + value
-            if factor is not None:
-                value = factor * value
+            value = factor * (COEF_ONE * left[where, h(j)].astype(jnp.float32) + value)
             out[where, h(j)] = value.astype(BF)
 
         def after_head():
@@ -586,19 +571,39 @@
         def right(j):
             return m[:, at(j, BLOCK)]
 
-        product(left, k, right, emit, after_head, after_cross, after_all)
-
-    square(a, None, 0, COEF_THREE * alpha, COEF_FIVE * alpha * alpha)
-    times(a, None, b, 0, alpha)
-    x1[:, mine] = (scale * (COEF_ONE * x0[:, mine].astype(jnp.float32) + dot(x0[...], m[...]))).astype(BF)
-    turn_one = send_to(x1.at[:, mine], partner)
-    times(b, 0, c, 1, None)
-    square(c, 1, 1, COEF_THREE, COEF_FIVE)
-    times(c, None, b, 2, None)
-    turn_one.wait_recv()
-    x2[:, mine] = (COEF_ONE * x1[:, mine].astype(jnp.float32) + dot(x1[...], m[...])).astype(BF)
-    turn_two = send_to(x2.at[:, mine], partner)
-    times(b, 2, a, 3, None)
+        product(left, receive, right, emit, after_head, after_cross, after_all)
+
+    def x_swap(i, half):
+        ref = xall.at[i + 1, :, at(half, HALF)]
+        return pltpu.make_async_remote_copy(
+            src_ref=ref, dst_ref=ref, send_sem=xsend.at[i], recv_sem=xrecv.at[i], device_id=partner, device_id_type=MESH
+        )
+
+    def iteration(i, _):
+        left, following = pairs.at[i], pairs.at[1 - i]
+        opening = i == 0
+        weight = jnp.where(opening, alpha, 1.0)
+
+        def receive_later(step):
+            @pl.when(i == 1)
+            def _():
+                step(left, 1)
+
+        square(left, receive_later, i, COEF_THREE * weight, COEF_FIVE * weight * weight)
+        times(left, lambda step: None, b, 2 * i, weight)
+
+        @pl.when(i == 1)
+        def _():
+            x_swap(0, core).wait_send()
+            x_swap(0, other).wait_recv()
+
+        own = xall[i, :, mine].astype(jnp.float32)
+        xall[i + 1, :, mine] = (jnp.where(opening, scale, 1.0) * (COEF_ONE * own + dot(xall[i], m[...]))).astype(BF)
+        x_swap(i, core).start()
+        times(b, lambda step: step(b, 2 * i), following, 2 * i + 1, 1.0)
+        return 0
+
+    lax.fori_loop(0, 2, iteration, 0)
 
     def some(block, low, high):
         close = spot(core * HALF + block * 256, 256, 256)
@@ -620,7 +625,9 @@
     some(ahead, 0, 2)
     receive_square(a, 3)
     some(ahead, 2, 4)
-    turn_two.wait_recv()
+    x_swap(1, core).wait_send()
+    x_swap(1, other).wait_recv()
+    x2 = xall.at[2]
     final[2] = last(pl.ds(0, rows), ahead)
     to_ahead = pltpu.make_async_remote_copy(
         src_ref=final.at[2], dst_ref=final.at[4 + core], send_sem=sems.at[COPIES], recv_sem=recvs.at[COPIES + core],
@@ -705,8 +712,7 @@
         scratch_shapes=[
             full(2, 2, rows, width), full(2, rows_b, width_b), full(2, rows, width), full(rows_b, width_b),
             buf(2, rows, width), buf(rows_b, width_b), dma((9,)), dma((6,)),
-            buf(N, N), buf(N, N), buf(N, N), buf(N, HALF),
-            buf(2 * rows, N), buf(2 * rows_b, NB), buf(2 * rows, N), buf(2 * rows, N), buf(7, rows, 256),
+            buf(2, N, N), buf(N, N), buf(N, HALF), buf(3, 2 * rows, N), buf(2 * rows_b, NB), buf(7, rows, 256),
             buf(2, 2, rows, 256), buf(2, rows, 256),
             buf(2, rows, width), buf(2, rows, width), buf(rows_b, width_b), buf(rows_b, width_b),
             buf(2, 256, 1280), buf(2, 2, 3, 64, 640), buf(2, 2, 64, 640), buf(2, 2, 3, 16, 640),
@@ -714,7 +720,7 @@
             buf(128, NB), buf(2, 3, 16, NB), buf(2, 16, NB), buf(2, 3, 16, 256), buf(8, 128, NB),
             buf(NB, NB), buf(NB, NB), buf(NB, NB),
             buf(2, BLOCK, BLOCK),
-            dma((COPIES + 2,)), dma((COPIES + 2,)), dma((7, 5)), dma((7, 5)),
+            dma((COPIES + 2,)), dma((COPIES + 2,)), dma((7, 5)), dma((7, 5)), dma((2,)), dma((2,)),
         ],
         compiler_params=pltpu.CompilerParams(collective_id=0, has_side_effects=True, vmem_limit_bytes=62 * 1024 * 1024),
     )(args[0], args[3], args[6], args[1], args[4], args[7])

time: 135 us -> 133 us (0.985)
  Pallas kernels: 134 us -> 132 us
    pallas_call x1, Pallas kernels: 132 us -> 130 us  [local(): pl.pallas_call(kernel, out_shape=outs, in_specs=[anywhere] * 6, out_specs...]
where the time goes in v9:
time: 133 us
  Pallas kernels  132 us (99%)
    pallas_call x1, Pallas kernels, local(): pl.pallas_call(kernel, out_shape=outs, in_specs=[anywhere] * 6, out_specs...  130 us

profile of v9, /device:TPU:1, one launch (start us, length us, event | category | flops | bytes accessed | tf_op | source)
XLA Modules:
  0.0 133.0 jit_solution(18380938272735927433)
XLA Ops:
  0.6 129.7 %shard_map.136 = (f32[176,512]{1,0:T(8,128)}, f32[176,512]{1,0:T(8,128)}, f32[64,256]{1,0:T(8,128)}, bf16[176,512]{1,0:T(8,128)(2,1)}, bf16[176,512]{1,0:T(8,128)(2,1)}, /*index=5*/bf16[64,256]{1,0:T(8,128)(2,1)}) custom-call(f32[1,352,512]{2,1,0:T(8,128)} %gate_g.1, f32[1,352,512]{2,1,0:T(8,128)} %up_g.1, f32[1,128,256]{2,1,0:T(8,128)} %branch_g.1, ...), custom_call_target="tpu_custom_call" | custom-call | tf_op jit(solution)/shard_map/pallas_call | solution.py:707
  130.4 2.4 %shard_map.137 = (f32[176,512]{1,0:T(8,128)}, f32[176,512]{1,0:T(8,128)}, f32[176,512]{1,0:T(8,128)}, f32[176,512]{1,0:T(8,128)}, f32[64,256]{1,0:T(8,128)}, /*index=5*/f32[64,256]{1,0:T(8,128)}) custom-call(f32[176,512]{1,0:T(8,128)} %get-tuple-element.12.refs_0_, f32[176,512]{1,0:T(8,128)} %get-tuple-element.13.refs_1_, ...), custom_call_target="tpu_custom_call" | custom-call | tf_op jit(solution)/shard_map/pallas_call | solution.py:729

commit v10 on v9

--- a/solution.py
+++ b/solution.py
@@ -380,10 +380,9 @@
         forward_b += [send_to(b_large(p, lax.rem(ring.index + k, 4)), partner) for k in (0, 3, 1)]
     for ring in small:
         ring.second()
-    for ring in small:
-        ring.finish()
-    for ring in large:
-        ring.start()
+    for near_ring, wide_ring in zip(small, large):
+        near_ring.finish()
+        wide_ring.start()
     for p, ring in enumerate(large_b):
         ring.finish()
         forward_b.append(send_to(b_large(p, lax.rem(ring.index + 2, 4)), partner))
@@ -518,17 +517,25 @@
             square_out(left, k, q, core).wait_send()
             square_out(left, k, q, other).wait_recv()
 
-    def product(left, receive, right, emit, after_head, after_cross, after_all):
+    def product(left, receive, right, emit, order, after_head, after_cross, after_last):
+        def head():
+            emit(at(core, HALF), 0, dot(left[at(core, HALF), :], right(0)))
+            after_head()
+
+        def cross():
+            receive(receive_square)
+            for q in range(2):
+                j = flip(q)
+                emit(o(q), j, dot(left[o(q), :], right(j)))
+                after_cross(q)
+
+        def corner():
+            emit(h(1), 1, dot(left[h(1), :], right(1)))
+            after_last()
+
         receive(receive_cross)
-        emit(at(core, HALF), 0, dot(left[at(core, HALF), :], right(0)))
-        after_head()
-        receive(receive_square)
-        for q in range(2):
-            j = flip(q)
-            emit(o(q), j, dot(left[o(q), :], right(j)))
-            after_cross(q)
-        emit(h(1), 1, dot(left[h(1), :], right(1)))
-        after_all()
+        for name in order:
+            {"head": head, "cross": cross, "last": corner}[name]()
 
     def square(left, receive, k_out, low, high):
         def emit(where, j, value):
@@ -544,14 +551,14 @@
         def right(j):
             return left[:, h(j)]
 
-        product(left, receive, right, emit, after_head, after_cross, lambda: None)
+        product(left, receive, right, emit, ("last", "cross", "head"), after_head, after_cross, lambda: None)
         for q in range(2):
             copy = stage_out(k_out, q)
             copy.wait_send()
             copy.wait_recv()
             m[o(flop(q)), at(q, BLOCK)] = stage[q].T
 
-    def times(left, receive, out, k_out, factor):
+    def times(left, receive, out, k_out, factor, order):
         def emit(where, j, value):
             value = factor * (COEF_ONE * left[where, h(j)].astype(jnp.float32) + value)
             out[where, h(j)] = value.astype(BF)
@@ -571,7 +578,7 @@
         def right(j):
             return m[:, at(j, BLOCK)]
 
-        product(left, receive, right, emit, after_head, after_cross, after_all)
+        product(left, receive, right, emit, order, after_head, after_cross, after_all)
 
     def x_swap(i, half):
         ref = xall.at[i + 1, :, at(half, HALF)]
@@ -590,7 +597,9 @@
                 step(left, 1)
 
         square(left, receive_later, i, COEF_THREE * weight, COEF_FIVE * weight * weight)
-        times(left, lambda step: None, b, 2 * i, weight)
+        times(left, lambda step: None, b, 2 * i, weight, ("cross", "head", "last"))
+
+        times(b, lambda step: step(b, 2 * i), following, 2 * i + 1, 1.0, ("head", "cross", "last"))
 
         @pl.when(i == 1)
         def _():
@@ -600,7 +609,6 @@
         own = xall[i, :, mine].astype(jnp.float32)
         xall[i + 1, :, mine] = (jnp.where(opening, scale, 1.0) * (COEF_ONE * own + dot(xall[i], m[...]))).astype(BF)
         x_swap(i, core).start()
-        times(b, lambda step: step(b, 2 * i), following, 2 * i + 1, 1.0)
         return 0
 
     lax.fori_loop(0, 2, iteration, 0)

time: 133 us -> 132 us (level)
  no operation moved by 1% of the time
where the time goes in v10:
time: 132 us
  Pallas kernels  131 us (99%)
    pallas_call x1, Pallas kernels, local(): pl.pallas_call(kernel, out_shape=outs, in_specs=[anywhere] * 6, out_specs...  129 us

profile of v10, /device:TPU:1, one launch (start us, length us, event | category | flops | bytes accessed | tf_op | source)
XLA Modules:
  0.0 131.9 jit_solution(7717540837169158209)
XLA Ops:
  0.6 128.7 %shard_map.136 = (f32[176,512]{1,0:T(8,128)}, f32[176,512]{1,0:T(8,128)}, f32[64,256]{1,0:T(8,128)}, bf16[176,512]{1,0:T(8,128)(2,1)}, bf16[176,512]{1,0:T(8,128)(2,1)}, /*index=5*/bf16[64,256]{1,0:T(8,128)(2,1)}) custom-call(f32[1,352,512]{2,1,0:T(8,128)} %gate_g.1, f32[1,352,512]{2,1,0:T(8,128)} %up_g.1, f32[1,128,256]{2,1,0:T(8,128)} %branch_g.1, ...), custom_call_target="tpu_custom_call" | custom-call | tf_op jit(solution)/shard_map/pallas_call | solution.py:715
  129.3 2.4 %shard_map.137 = (f32[176,512]{1,0:T(8,128)}, f32[176,512]{1,0:T(8,128)}, f32[176,512]{1,0:T(8,128)}, f32[176,512]{1,0:T(8,128)}, f32[64,256]{1,0:T(8,128)}, /*index=5*/f32[64,256]{1,0:T(8,128)}) custom-call(f32[176,512]{1,0:T(8,128)} %get-tuple-element.12.refs_0_, f32[176,512]{1,0:T(8,128)} %get-tuple-element.13.refs_1_, ...), custom_call_target="tpu_custom_call" | custom-call | tf_op jit(solution)/shard_map/pallas_call | solution.py:737

commit v11 on v10

--- a/solution.py
+++ b/solution.py
@@ -273,15 +273,18 @@
             self.index, self.block, self.cut = index, block, cut
 
         def start(self):
-            ref = self.block(self.index)
-            self.right = send_to(ref, self.next)
-            self.left = send_to(ref, self.prev)
+            self.right = [send_to(self.cut(self.index, half), self.next) for half in (0, 1)]
+            self.left = [send_to(self.cut(self.index, half), self.prev) for half in (1, 0)]
 
         def second(self):
-            self.right.wait_recv()
+            self.right[0].wait_recv()
             self.far = [send_to(self.cut(lax.rem(self.index + 3, 4), 0), self.next)]
-            self.left.wait_recv()
+            self.left[0].wait_recv()
             self.far.append(send_to(self.cut(lax.rem(self.index + 1, 4), 1), self.prev))
+
+        def third(self):
+            self.right[1].wait_recv()
+            self.left[1].wait_recv()
 
         def finish(self):
             for copy in self.far:
@@ -359,6 +362,7 @@
     twos = [scatter_two(0), scatter_two(1)]
     for ring in small_b:
         ring.second()
+        ring.third()
     swaps = []
     for p in range(2):
         i2 = axes[p][1][1]
@@ -375,11 +379,14 @@
         copy.wait_recv()
         ring.start()
     forward_b, forward = [], []
+    for ring in large_b:
+        ring.second()
     for p, ring in enumerate(large_b):
-        ring.second()
+        ring.third()
         forward_b += [send_to(b_large(p, lax.rem(ring.index + k, 4)), partner) for k in (0, 3, 1)]
     for ring in small:
         ring.second()
+        ring.third()
     for near_ring, wide_ring in zip(small, large):
         near_ring.finish()
         wide_ring.start()
@@ -426,12 +433,15 @@
         g_b[at(i, 128), :] = gram_b[i]
     square_b(g_b, COEF_THREE * alpha_b, COEF_FIVE * alpha_b * alpha_b)
     times_b(g_b, t_b, alpha_b)
+    for p, ring in enumerate(large):
+        ring.second()
+        forward.append(send_to(g_large(p, ring.index), partner))
     line_b = rows_of(xb[at(core, rows_b), :], scale_b)
     times_b(t_b, g_b, 1.0)
     square_b(g_b, COEF_THREE, COEF_FIVE)
     for p, ring in enumerate(large):
-        ring.second()
-        forward += [send_to(g_large(p, lax.rem(ring.index + k, 4)), partner) for k in (0, 3, 1)]
+        ring.third()
+        forward += [send_to(g_large(p, lax.rem(ring.index + k, 4)), partner) for k in (3, 1)]
     times_b(g_b, t_b, 1.0)
     line_b = rows_of(line_b, 1.0)
     times_b(t_b, g_b, 1.0)

time: 132 us -> 131 us (level)
  no operation moved by 1% of the time
where the time goes in v11:
time: 131 us
  Pallas kernels  130 us (99%)
    pallas_call x1, Pallas kernels, local(): pl.pallas_call(kernel, out_shape=outs, in_specs=[anywhere] * 6, out_specs...  128 us

profile of v11, /device:TPU:1, one launch (start us, length us, event | category | flops | bytes accessed | tf_op | source)
XLA Modules:
  0.0 131.1 jit_solution(6454780225740412850)
XLA Ops:
  0.6 127.9 %shard_map.136 = (f32[176,512]{1,0:T(8,128)}, f32[176,512]{1,0:T(8,128)}, f32[64,256]{1,0:T(8,128)}, bf16[176,512]{1,0:T(8,128)(2,1)}, bf16[176,512]{1,0:T(8,128)(2,1)}, /*index=5*/bf16[64,256]{1,0:T(8,128)(2,1)}) custom-call(f32[1,352,512]{2,1,0:T(8,128)} %gate_g.1, f32[1,352,512]{2,1,0:T(8,128)} %up_g.1, f32[1,128,256]{2,1,0:T(8,128)} %branch_g.1, ...), custom_call_target="tpu_custom_call" | custom-call | tf_op jit(solution)/shard_map/pallas_call | solution.py:725
  128.5 2.4 %shard_map.137 = (f32[176,512]{1,0:T(8,128)}, f32[176,512]{1,0:T(8,128)}, f32[176,512]{1,0:T(8,128)}, f32[176,512]{1,0:T(8,128)}, f32[64,256]{1,0:T(8,128)}, /*index=5*/f32[64,256]{1,0:T(8,128)}) custom-call(f32[176,512]{1,0:T(8,128)} %get-tuple-element.12.refs_0_, f32[176,512]{1,0:T(8,128)} %get-tuple-element.13.refs_1_, ...), custom_call_target="tpu_custom_call" | custom-call | tf_op jit(solution)/shard_map/pallas_call | solution.py:747
